TPU v7x, 512 devices: a whole 4x8x8 slice. The times are simulated.
512 devices in a mesh: sp: 64 (over z, y), tp: 8 (over x, core).
Axes of the slice: x: 4, y: 8, z: 8, core: 2. Of those that a mesh axis runs over, the one named last changes fastest.
Arguments:
- residual: bfloat16 [8192, 2048], P('sp', 'tp'), may hold values from -24 to 24
- queries: bfloat16 [8192, 2048], P('sp', 'tp'), may hold values from -16 to 16
- key_proj: bfloat16 [8192, 512], P(('sp', 'tp')), may hold values from -8 to 8
- value_proj: bfloat16 [8192, 512], P(('sp', 'tp')), may hold values from -6 to 6
- diff_lambda: float32 [8], replicated, may hold values from 0.3 to 0.8
- head_gain: float32 [256], replicated, may hold values from 0.1 to 1.9
- out_weight: bfloat16 [2048, 2048], P(None, 'tp'), may hold values from -0.125 to 0.125
- norm_gain: float32 [2048], P('tp'), may hold values from 0.1 to 1.9
- up_weight: bfloat16 [2048, 8192], P('sp', 'tp'), may hold values from -0.125 to 0.125
- down_weight: bfloat16 [8192, 2048], P('tp', 'sp'), may hold values from -0.0625 to 0.0625
Outputs:
- layer_out: bfloat16 [8192, 2048], P('sp', 'tp')
All inputs are finite; a program needn't handle non-finite values.
Results may differ from a plain program's by a relative error of at most 0.012.
Values may be sent and summed in bfloat16 or wider, within the bound.
A program may use at most 64 MiB of HBM per device.

v0:
```python
import jax
import jax.numpy as jnp
from jax import lax
from jax.sharding import PartitionSpec as P

D = 2048
HEADS = 8
KV_HEADS = 2
HEAD_DIM = 128
VALUE_DIM = 256


epsilon = 1e-06


def turned_gather(arrays, axis, dims):
    turned = [jnp.moveaxis(a, dim, 0) for a, dim in zip(arrays, dims)]
    both = jnp.concatenate([t.reshape(len(t), -1) for t in turned], axis=1)
    whole, at, finished = (lax.all_gather(both, axis, axis=0, tiled=True), 0, [])
    for t, dim in zip(turned, dims):
        share = whole[:, at : at + t[0].size].reshape(-1, *t.shape[1:])
        finished.append(jnp.moveaxis(share, 0, dim))
        at += t[0].size
    return tuple(finished)


def from_everyone(shard, axis):
    copies = jnp.broadcast_to(shard, (lax.axis_size(axis), *shard.shape))
    return lax.all_to_all(copies, axis, split_axis=0, concat_axis=0, tiled=True)


def laid_out(parts, dim):
    dims = list(parts.shape[1:])
    dims[dim] *= parts.shape[0]
    return jnp.moveaxis(parts, 0, dim).reshape(dims)


def collect(shard, axis, dim):
    parts = from_everyone(shard, axis)
    return laid_out(parts, dim)


def sent_together(arrays, axis, dim, along):
    ends, at = ([], 0)
    for a in arrays[:-1]:
        at += a.shape[along]
        ends.append(at)
    both = jnp.concatenate(arrays, axis=along)
    return tuple(jnp.split(lax.all_gather(both, axis, axis=dim, tiled=True), ends, axis=along))


def side_by_side(arrays, axis, split_dim, concat_dim, along):
    columns = [a.reshape(*a.shape[:along], -1) for a in arrays]
    both = jnp.concatenate(columns, axis=along)
    whole, at, finished = (
        lax.all_to_all(both, axis, split_axis=split_dim, concat_axis=concat_dim, tiled=True),
        0,
        [],
    )
    for a, column in zip(arrays, columns):
        share = whole[..., at : at + column.shape[along]]
        finished.append(share.reshape(*share.shape[:along], *a.shape[along:]))
        at += column.shape[along]
    return tuple(finished)


def over_copies(shard, axis):
    everything = from_everyone(shard, axis)
    return jnp.sum(everything, axis=0)


def split_up(shard, dim, length):
    dims = shard.shape
    parts = shard.reshape(*dims[:dim], length, dims[dim] // length, *dims[dim + 1 :])
    return jnp.moveaxis(parts, dim, 0)


def sent_and_summed(shard, axis, dim):
    parts = split_up(shard, dim, lax.axis_size(axis))
    arrived = lax.all_to_all(parts, axis, split_axis=0, concat_axis=0, tiled=True)
    return arrived.sum(axis=0)


def head_norm(per_map, lambdas, gain):
    difference = per_map[:, 0] - lambdas[:, None, None] * per_map[:, 1]
    scaled = (
        difference
        * lax.rsqrt(jnp.mean(difference * difference, axis=-1, keepdims=True) + epsilon)
        * gain
    )
    return scaled.astype(jnp.bfloat16)


def on_device(
    residual,
    queries,
    key_proj,
    value_proj,
    diff_lambda,
    head_gain,
    out_weight,
    norm_gain,
    up_weight,
    down_weight,
):
    up_whole, down_whole = turned_gather((up_weight, down_weight), "sp", (0, 1))
    rows_here = residual.shape[0]
    per_group = HEADS // KV_HEADS
    scaling = HEAD_DIM ** (-0.5)
    all_queries = collect(queries, "tp", 1)
    query_grid = all_queries.reshape(rows_here, KV_HEADS, per_group, 2, HEAD_DIM)
    stat_shape = (KV_HEADS, per_group, 2, rows_here)
    maxima = jnp.full(stat_shape, -1e30, jnp.float32)
    key_piece, value_piece = sent_together((key_proj, value_proj), "sp", 0, 1)
    key_count = key_piece.shape[0]
    key_grid = key_piece.reshape(key_count, KV_HEADS, 2, HEAD_DIM)
    value_grid = value_piece.reshape(key_count, KV_HEADS, VALUE_DIM)
    scores = (
        jnp.einsum("qagcd,kacd->agcqk", query_grid, key_grid, preferred_element_type=jnp.float32)
        * scaling
    )
    highest = jnp.maximum(maxima, jnp.max(scores, axis=-1))
    weights = jnp.exp(scores - highest[..., None])
    totals = jnp.sum(weights, axis=-1)
    weighted = jnp.einsum(
        "agcqk,kae->agcqe",
        weights.astype(jnp.bfloat16),
        value_grid,
        preferred_element_type=jnp.float32,
    )
    maxima, totals, weighted = (highest, totals, weighted)
    maxima = maxima.reshape(HEADS, 2, rows_here)
    totals = totals.reshape(HEADS, 2, rows_here)
    weighted = weighted.reshape(HEADS, 2, rows_here, VALUE_DIM)
    tp_size = lax.axis_size("tp")
    local_heads = HEADS // tp_size
    got_max, got_tot, got_sum = side_by_side((maxima, totals, weighted), "tp", 0, 0, 3)
    got_max = got_max.reshape(tp_size, local_heads, 2, rows_here)
    got_tot = got_tot.reshape(tp_size, local_heads, 2, rows_here)
    got_sum = got_sum.reshape(tp_size, local_heads, 2, rows_here, VALUE_DIM)
    highest = jnp.max(got_max, axis=0)
    factor = jnp.exp(got_max - highest)
    totals_all = jnp.sum(factor * got_tot, axis=0)
    sums_all = jnp.sum(factor[..., None] * got_sum, axis=0)
    lambdas = lax.dynamic_slice_in_dim(diff_lambda, lax.axis_index("tp") * local_heads, local_heads)
    own_heads = head_norm(sums_all / totals_all[..., None], lambdas, head_gain)
    head_outputs = collect(own_heads, "tp", 0)
    out_grid = out_weight.reshape(HEADS, VALUE_DIM, out_weight.shape[1])
    projected = jnp.einsum(
        "hqe,hed->qd", head_outputs, out_grid, preferred_element_type=jnp.float32
    )
    after_mix = residual.astype(jnp.float32) + projected
    squares = over_copies(jnp.sum(after_mix * after_mix, axis=1), "tp")
    normed = (after_mix * lax.rsqrt(squares / D + epsilon)[:, None] * norm_gain).astype(
        jnp.bfloat16
    )
    full_rows = collect(normed, "tp", 1)
    hidden = jnp.dot(full_rows, up_whole, preferred_element_type=jnp.float32)
    activated = jnp.square(jax.nn.relu(hidden)).astype(jnp.bfloat16)
    partial_value = jnp.dot(activated, down_whole, preferred_element_type=jnp.float32)
    mixer_sum = sent_and_summed(partial_value, "tp", 1)
    return (after_mix + mixer_sum).astype(jnp.bfloat16)


def solution(mesh):
    return jax.shard_map(
        on_device,
        mesh=mesh,
        in_specs=(
            P("sp", "tp"),
            P("sp", "tp"),
            P(("sp", "tp"), None),
            P(("sp", "tp"), None),
            P(),
            P(),
            P(None, "tp"),
            P("tp"),
            P("sp", "tp"),
            P("tp", "sp"),
        ),
        out_specs=P("sp", "tp"),
        check_vma=False,
    )
```

profile of v0, /device:TPU:1, one launch (start us, length us, event | category | flops | bytes accessed | tf_op | source)
XLA Modules:
  0.0 231.3 jit_solution(17370695818168791017)
XLA Ops:
  6.5 0.0 copy-start
  6.5 0.0 all-gather.3.cloned.1.call-start
  6.5 1.4 pad_maximum_fusion.2
  8.0 0.0 all-gather.3.cloned.1.call-update
  8.0 0.0 all-gather.5.cloned.1.call-start
  8.1 1.5 pad_maximum_fusion.1
  9.6 0.0 all-gather.5.cloned.1.call-update
  9.6 1.0 copy.62
  10.6 0.9 broadcast_in_dim.10
  11.4 10.9 %all-to-all-start = ((bf16[8,128,256]{1,2,0:T(8,128)(2,1)}), bf16[8,128,256]{1,2,0:T(8,128)(2,1)}, u32[]{:S(2)}, u32[]{:S(2)}) async-start(bf16[8,128,256]{1,2,0:T(8,128)(2,1)} %broadcast_in_dim.10), calls=%async_computation | async-start | bytes 1048576 | tf_op jit(solution)/shard_map/all_to_all | solution.py:29
  22.3 72.8 %all-gather.3.cloned.1.call-done = bf16[1024,1024]{1,0:T(8,128)(2,1)} async-done(((bf16[16,1024]{1,0:T(8,128)(2,1)}), bf16[1024,1024]{1,0:T(8,128)(2,1)}) %all-gather.3.cloned.1.call-update) | async-done | bytes 2097168 | tf_op jit(solution)/shard_map/all_gather | solution.py:49
  95.1 1.7 fusion.34
  96.8 1.4 copy.93
  98.2 0.5 copy.92
  98.7 0.0 all-to-all-done
  98.7 2.3 %bitcast_reduce_fusion = (f32[2,4,2,128]{3,1,2,0:T(4,128)S(1)}, f32[2,2,1024,128,4]{3,2,4,1,0:T(8,128)S(1)}) fusion(bf16[1024,2,2,128,1]{0,3,4,2,1:T(8,128)(2,1)S(1)} %bitcast.73, bf16[128,2,4,2,128]{0,4,3,2,1:T(8,128)(2,1)} %bitcast.3), kind=kOutput, calls=%fused_computation.1 | convolution fusion | flops 541063168 | bytes 9969664 | tf_op jit(solution)/shard_map/qagcd,kacd->agcqk/dot_general | solution.py:119
  101.1 0.0 copy-start.1
  101.1 1.8 fusion.2
  102.9 0.0 copy-done.1
  102.9 3.2 %fusion.7 = f32[2,4,2,128,256]{4,3,2,1,0:T(8,128)} fusion(bf16[1024,2,256,1,1]{0,2,4,3,1:T(8,128)(2,1)S(1)} %bitcast.75, bf16[2,4,2,128,1024]{3,4,1,2,0:T(8,128)(2,1)S(1)} %get-tuple-element.8), kind=kOutput, calls=%fused_computation.9 | convolution fusion | flops 1073741824 | bytes 7340032 | tf_op jit(solution)/shard_map/agcqk,kae->agcqe/dot_general | solution.py:125
  106.0 2.8 %copy.72 = f32[8,2,128,256]{2,1,3,0:T(2,128)S(1)} copy(f32[8,2,128,256]{3,2,1,0:T(8,128)} %bitcast.74) | data formatting | bytes 4194304 | tf_op jit(solution)/shard_map/reshape | solution.py:134
  108.9 0.0 copy-start.5
  108.9 2.1 pad_maximum_fusion
  111.0 9.4 %all-to-all-start.1 = ((f32[8,2,128,258]{2,1,3,0:T(2,128)}), f32[8,2,128,258]{2,1,3,0:T(2,128)S(1)}, u32[]{:S(2)}, u32[]{:S(2)}) async-start(f32[8,2,128,258]{2,1,3,0:T(2,128)} %pad_maximum_fusion), calls=%async_computation.1 | async-start | bytes 4227072 | tf_op jit(solution)/shard_map/all_to_all | solution.py:56
  120.4 0.0 copy-done.5
  120.4 0.6 dynamic_slice.3
  121.0 25.8 %all-to-all-done.1 = f32[8,2,128,258]{2,1,3,0:T(2,128)S(1)} async-done(((f32[8,2,128,258]{2,1,3,0:T(2,128)}), f32[8,2,128,258]{2,1,3,0:T(2,128)S(1)}, u32[]{:S(2)}, u32[]{:S(2)}) %all-to-all-start.1) | async-done | bytes 2113568 | tf_op jit(solution)/shard_map/all_to_all | solution.py:56
  146.9 1.0 fusion.9
  147.8 0.1 bitcast_divide_fusion
  147.9 0.9 multiply_reduce_fusion.1
  148.9 0.0 copy-done.3
  148.9 0.1 multiply_convert_fusion.1
  149.0 0.1 copy.77
  149.2 12.8 %all_to_all.31 = bf16[8,1,128,256]{3,2,1,0:T(8,128)(2,1)S(1)} all-to-all(bf16[8,1,128,256]{3,2,1,0:T(8,128)(2,1)S(1)} %broadcast_in_dim.12), channel_id=1, replica_groups=mesh['sp'=64,'tp'=8] {'tp'}, dimensions={0} | all-to-all | bytes 1048576 | tf_op jit(solution)/shard_map/all_to_all | solution.py:29
  161.9 0.0 copy-done
  161.9 0.0 copy-done.2
  161.9 0.4 multiply_reduce_fusion
  162.3 8.0 %all_to_all.32 = f32[8,1,128]{2,1,0:T(1,128)S(1)} all-to-all(f32[8,1,128]{2,1,0:T(1,128)S(1)} %broadcast_in_dim.13), channel_id=1, replica_groups=mesh['sp'=64,'tp'=8] {'tp'}, dimensions={0} | all-to-all | bytes 8192 | tf_op jit(solution)/shard_map/all_to_all | solution.py:29
  170.4 0.1 multiply_convert_fusion
  170.5 0.1 copy.79
  170.6 0.1 broadcast_in_dim.28
  170.7 12.4 %all_to_all.33 = bf16[8,128,256]{1,2,0:T(8,128)(2,1)S(1)} all-to-all(bf16[8,128,256]{1,2,0:T(8,128)(2,1)S(1)} %broadcast_in_dim.28), channel_id=1, replica_groups=mesh['sp'=64,'tp'=8] {'tp'}, dimensions={0} | all-to-all | bytes 1048576 | tf_op jit(solution)/shard_map/all_to_all | solution.py:29
  183.1 15.0 %all-gather.5.cloned.1.call-done = bf16[2048,2048]{1,0:T(8,128)(2,1)} async-done(((bf16[32,2048]{1,0:T(8,128)(2,1)}), bf16[2048,2048]{1,0:T(8,128)(2,1)}) %all-gather.5.cloned.1.call-update) | async-done | bytes 8388624 | tf_op jit(solution)/shard_map/all_gather | solution.py:19
  198.1 5.6 %fusion.3 = f32[128,2048]{1,0:T(8,128)S(1)} fusion(bf16[2048,2048]{1,0:T(8,128)(2,1)} %all-gather.5.cloned.1.call-done, bf16[128,2048]{0,1:T(8,128)(2,1)S(1)} %bitcast.78), kind=kOutput, calls=%fused_computation.5 | convolution fusion | flops 1074135040 | bytes 9961472 | tf_op jit(solution)/shard_map/dot_general | solution.py:160
  203.7 0.1 copy.112
  203.8 19.9 %all_to_all.34 = f32[8,128,256]{2,1,0:T(8,128)S(1)} all-to-all(f32[8,128,256]{2,1,0:T(8,128)S(1)} %bitcast.72), channel_id=1, replica_groups=mesh['sp'=64,'tp'=8] {'tp'}, dimensions={0} | all-to-all | bytes 2097152 | tf_op jit(solution)/shard_map/all_to_all | solution.py:80
  223.7 0.1 reduce_sum.72
  223.8 0.6 add_convert_fusion
  (18 shorter events, 0.2 us)
Async XLA Ops:
  6.5 155.4 %copy-start = (bf16[2048,256]{1,0:T(8,128)(2,1)S(1)}, bf16[2048,256]{1,0:T(8,128)(2,1)}, u32[]{:S(2)}) copy-start(bf16[2048,256]{1,0:T(8,128)(2,1)} %param.16) | copy-start | bytes 3145732
  6.5 88.5 %all-gather.3.cloned.1.call-start = ((), (), s32[]{:S(2)}) async-start(), calls=%async_computation.6 | async-start | bytes 2129920 | tf_op jit(solution)/shard_map/all_gather | solution.py:49
  8.0 190.1 %all-gather.5.cloned.1.call-start = ((), (), s32[]{:S(2)}) async-start(), calls=%async_computation.7 | async-start | bytes 8519680 | tf_op jit(solution)/shard_map/all_gather | solution.py:19
  11.4 87.2 %all-to-all-start = ((bf16[8,128,256]{1,2,0:T(8,128)(2,1)}), bf16[8,128,256]{1,2,0:T(8,128)(2,1)}, u32[]{:S(2)}, u32[]{:S(2)}) async-start(bf16[8,128,256]{1,2,0:T(8,128)(2,1)} %broadcast_in_dim.10), calls=%async_computation | async-start | bytes 1048576 | tf_op jit(solution)/shard_map/all_to_all | solution.py:29
  101.1 1.8 copy-start.1
  108.9 11.5 %copy-start.5 = (f32[8]{0:T(128)S(1)}, f32[8]{0:T(128)}, u32[]{:S(2)}) copy-start(f32[8]{0:T(128)} %param.14) | copy-start | bytes 100
  111.0 37.9 %copy-start.3 = (f32[256]{0:T(256)S(1)}, f32[256]{0:T(256)}, u32[]{:S(2)}) copy-start(f32[256]{0:T(256)} %param.15) | copy-start | bytes 3076
  111.0 50.9 %copy-start.2 = (bf16[128,256]{1,0:T(8,128)(2,1)S(1)}, bf16[128,256]{1,0:T(8,128)(2,1)}, u32[]{:S(2)}) copy-start(bf16[128,256]{1,0:T(8,128)(2,1)} %param.10) | copy-start | bytes 196612
  111.0 35.8 %all-to-all-start.1 = ((f32[8,2,128,258]{2,1,3,0:T(2,128)}), f32[8,2,128,258]{2,1,3,0:T(2,128)S(1)}, u32[]{:S(2)}, u32[]{:S(2)}) async-start(f32[8,2,128,258]{2,1,3,0:T(2,128)} %pad_maximum_fusion), calls=%async_computation.1 | async-start | bytes 4227072 | tf_op jit(solution)/shard_map/all_to_all | solution.py:56
  120.4 50.0 %copy-start.4 = (f32[256]{0:T(256)S(1)}, f32[256]{0:T(256)}, u32[]{:S(2)}) copy-start(f32[256]{0:T(256)} %param.17) | copy-start | bytes 3076
Sparse Core Ops, SparseCore 0:
  10.4 84.6 all-gather.2
  98.1 99.9 all-gather.4
where the time goes:
time: 232 us; the launch traced here: 231 us
  waiting for transfers between devices  114 us (49%)
  blocking collectives  53.1 us (23%)
  starting transfers between devices  20.3 us (9%)
  between operations  13.6 us (6%)
  matrix products  11.5 us (5%)
  other arithmetic  9.83 us (4%)
  local copies, waits for them, and re-layouts  9.31 us (4%)
    all_gather x1, waiting for transfers between devices, sent_together(): lax.all_gather(both, axis, axis=dim, tiled=True)  72.8 us
    all_to_all x3, blocking collectives, from_everyone(): return lax.all_to_all(copies, axis, split_axis=0, concat_axis=0, tiled=True)  33.2 us
    all_to_all x1, waiting for transfers between devices, side_by_side(): lax.all_to_all(both, axis, split_axis=split_dim, concat_axis=concat_dim,...  25.8 us
    all_to_all x1, blocking collectives, sent_and_summed(): lax.all_to_all(parts, axis, split_axis=0, concat_axis=0, tiled=True)  19.9 us
    all_gather x1, waiting for transfers between devices, turned_gather(): lax.all_gather(both, axis, axis=0, tiled=True)  15 us
    all_to_all x1, starting transfers between devices, from_everyone(): return lax.all_to_all(copies, axis, split_axis=0, concat_axis=0, tiled=True)  10.9 us
    all_to_all x1, starting transfers between devices, side_by_side(): lax.all_to_all(both, axis, split_axis=split_dim, concat_axis=concat_dim,...  9.39 us
    dot_general x1, matrix products, on_device(): jnp.dot(activated, down_whole, preferred_element_type=jnp.float32)  5.59 us
  transfers between devices with their start and end apart: 4, of which 3 were waited for; matrix products, arithmetic and copies ran while one was open for 10% of the time, Pallas kernels for 0%

commit v1 on v0

v1 whole, which is shorter than its diff:
```python
import jax
import jax.numpy as jnp
from jax import lax
from jax.experimental import pallas as pl
from jax.experimental.pallas import tpu as pltpu
from jax.sharding import PartitionSpec as P

D = 2048
HEADS = 8
HEAD_DIM = 128
VALUE_DIM = 256
RING = 8
TP = 8
ROWS = 128
EPSILON = 1e-06
MESH = pl.DeviceIdType.MESH
F32 = jnp.float32
BF16 = jnp.bfloat16
LOG_SCALE = HEAD_DIM ** (-0.5) * 1.4426950408889634
NT = (((1,), (1,)), ((), ()))


def wrap(i):
    return lax.rem(i + RING, RING)


class Gather:
    def __init__(self, first, second, y, z, tp, send, near, far):
        self.arrays = (first, second)
        self.y, self.z, self.tp = y, z, tp
        self.send, self.near, self.far = send, near, far

    def chunk(self, kind, p2, p1):
        array = self.arrays[kind]
        return array.at[p2 * RING + p1] if kind == 0 else array.at[p1 * RING + p2]

    def me1(self, kind):
        return self.y if kind == 0 else self.z

    def me2(self, kind):
        return self.z if kind == 0 else self.y

    def device(self, along_y, step):
        if along_y:
            return (self.z * RING + wrap(self.y + step), self.tp)
        return (wrap(self.z + step) * RING + self.y, self.tp)

    def near_copy(self, kind, way, s, at):
        c = self.chunk(kind, self.me2(kind), at)
        return pltpu.make_async_remote_copy(
            src_ref=c, dst_ref=c, send_sem=self.send.at[kind],
            recv_sem=self.near.at[kind, way, s],
            device_id=self.device(kind == 0, 1 - 2 * way), device_id_type=MESH)

    def far_copy(self, kind, way, s, at2, at1):
        c = self.chunk(kind, at2, at1)
        return pltpu.make_async_remote_copy(
            src_ref=c, dst_ref=c, send_sem=self.send.at[kind],
            recv_sem=self.far.at[kind, way, s, at1],
            device_id=self.device(kind == 1, 1 - 2 * way), device_id_type=MESH)

    def open_chunk(self, kind, at1):
        for way in range(2):
            self.far_copy(kind, way, 0, self.me2(kind), at1).start()

    def begin(self):
        for kind in range(2):
            for way in range(2):
                self.near_copy(kind, way, 0, self.me1(kind)).start()
        for kind in range(2):
            self.open_chunk(kind, self.me1(kind))

    def near_step(self, u):
        for way in range(2):
            if way == 1 and u == 4:
                continue
            for kind in range(2):
                at = wrap(self.me1(kind) - u * (1 - 2 * way))
                self.near_copy(kind, way, u - 1, at).wait_recv()
                if u < 4 - way:
                    self.near_copy(kind, way, u, at).start()
                self.open_chunk(kind, at)

    def far_step(self, s, j):
        half = lax.div(j + 1, 2)
        offset = half * (1 - 2 * lax.rem(j, 2))
        for way in range(2):
            mine = (j < 4) if way == 0 else (j >= 4)
            for kind in range(2):
                at1 = wrap(self.me1(kind) + offset)
                at2 = wrap(self.me2(kind) - s * (1 - 2 * way))

                def arrive():
                    self.far_copy(kind, way, s - 1, at2, at1).wait_recv()

                def forward():
                    self.far_copy(kind, way, s, at2, at1).start()

                if s < 4:
                    arrive()
                else:
                    pl.when(mine)(arrive)
                if s < 3:
                    forward()
                elif s == 3:
                    pl.when(mine)(forward)

    def far_steps(self, s, low, high):
        @pl.loop(low, high)
        def _(j):
            self.far_step(s, j)

    def finish(self):
        for kind in range(2):
            part = self.arrays[kind].at[0 : RING * RING - 1]
            pltpu.make_async_remote_copy(
                src_ref=part, dst_ref=part, send_sem=self.send.at[kind],
                recv_sem=self.near.at[kind, 0, 0],
                device_id=self.device(True, 1), device_id_type=MESH).wait_send()


def kernel(
    res_ref, q_ref, key_ref, val_ref, lam_ref, hgain_ref, ow_ref, ngain_ref, up_ref, down_ref,
    out_ref,
    k_all, v_all, up_all, dn_all, q_all, st_all, d_out, d_all, ho_all, an_all, sq_all,
    rs_out, rs_all, o_scr, am_scr, hid_scr,
    kv_send, kv_near, kv_far, w_send, w_near, w_far, x_send, x_recv,
):
    sp, tp = lax.axis_index("sp"), lax.axis_index("tp")
    z, y = lax.div(sp, RING), lax.rem(sp, RING)
    kv = Gather(k_all, v_all, y, z, tp, kv_send, kv_near, kv_far)
    w = Gather(up_all, dn_all, y, z, tp, w_send, w_near, w_far)

    barrier = pltpu.get_barrier_semaphore()

    @pl.loop(1, TP)
    def _(p):
        pl.semaphore_signal(barrier, inc=1, device_id=(sp, wrap(tp + p)), device_id_type=MESH)

    for along_y in (True, False):
        for step in (1, -1):
            pl.semaphore_signal(barrier, inc=1, device_id=kv.device(along_y, step), device_id_type=MESH)

    k_all[sp] = key_ref[...]
    v_all[sp] = val_ref[...]
    up_all[sp] = up_ref[...]
    rows = lax.broadcasted_iota(jnp.int32, (32, 32), 0)
    cols = lax.broadcasted_iota(jnp.int32, (32, 32), 1)
    eye = jnp.where(rows == cols, 1.0, 0.0).astype(BF16)
    dn_all[sp] = lax.dot_general(eye, down_ref[...], NT, preferred_element_type=F32).astype(BF16)
    q_all[tp] = q_ref[...]

    pl.semaphore_wait(barrier, TP - 1 + 4)

    def x_copy(k, src, dst, slot, peer):
        return pltpu.make_async_remote_copy(
            src_ref=src, dst_ref=dst.at[slot], send_sem=x_send.at[k], recv_sem=x_recv.at[k, slot],
            device_id=(sp, peer), device_id_type=MESH)

    def x_share(k, array):
        @pl.loop(1, TP)
        def _(p):
            x_copy(k, array.at[tp], array, tp, wrap(tp + p)).start()

    def x_wait(k, array):
        @pl.loop(1, TP)
        def _(p):
            slot = wrap(tp - p)
            x_copy(k, array.at[slot], array, slot, slot).wait_recv()

    def x_sent(k, array):
        part = array.at[0:7]
        pltpu.make_async_remote_copy(
            src_ref=part, dst_ref=part, send_sem=x_send.at[k], recv_sem=x_recv.at[k, 0],
            device_id=(sp, wrap(tp + 1)), device_id_type=MESH).wait_send()

    kv.begin()
    x_share(0, q_all)
    w.begin()
    for u in range(1, 5):
        kv.near_step(u)
    for s in range(1, 4):
        kv.far_steps(s, 0, 8)
        w.near_step(s)
    w.near_step(4)
    kv.far_steps(4, 0, 8)
    x_wait(0, q_all)

    lane = lax.broadcasted_iota(jnp.int32, (ROWS, 128), 1)

    def attend(gc, stats):
        g, c = lax.div(gc, 2), lax.rem(gc, 2)
        q = q_all[pl.ds(4 * g, 4), :, pl.ds(pl.multiple_of(c * 128, 128), 128)].reshape(4 * ROWS, 128)
        k = k_all[:, :, pl.ds(pl.multiple_of(gc * 128, 128), 128)].reshape(1024, 128)
        v = v_all[:, :, pl.ds(pl.multiple_of(g * 256, 256), 256)].reshape(1024, 256)
        s = lax.dot_general(q, k, NT, preferred_element_type=F32)
        m = jnp.max(s, axis=1, keepdims=True)
        p = jnp.exp2((s - m) * LOG_SCALE)
        t = jnp.sum(p, axis=1, keepdims=True)
        o = jnp.dot(p.astype(BF16), v, preferred_element_type=F32)
        m = m * LOG_SCALE
        for i in range(4):
            at = (4 * g + i) * 2 + c
            o_scr[at] = o[i * ROWS : (i + 1) * ROWS]
            stats = jnp.where(lane == at, m[i * ROWS : (i + 1) * ROWS], stats)
            stats = jnp.where(lane == at + 16, t[i * ROWS : (i + 1) * ROWS], stats)
        w.far_step(1, 2 * gc)
        w.far_step(1, 2 * gc + 1)
        return stats

    stats = lax.fori_loop(0, 4, attend, jnp.zeros((ROWS, 128), F32))
    st_all[tp] = jnp.transpose(stats)[0:32]
    w.far_steps(2, 0, 1)
    x_share(1, st_all)
    w.far_steps(2, 1, 3)
    x_wait(1, st_all)

    every = st_all[...]
    maxima, totals = every[:, 0:16], every[:, 16:32]
    highest = jnp.max(maxima, axis=0)
    total = jnp.sum(jnp.exp2(maxima - highest[None]) * totals, axis=0)
    mine = st_all[tp]
    coef = jnp.exp2(mine[0:16] - highest) / total
    row = lax.broadcasted_iota(jnp.int32, (16, 128), 0)
    factor = jnp.ones((16, 128), F32)
    for h in range(HEADS):
        factor = jnp.where(row == 2 * h + 1, -lam_ref[h], factor)
    coef = jnp.concatenate([coef * factor, jnp.zeros((112, 128), F32)], axis=0)
    coef = jnp.transpose(coef)
    for h in range(HEADS):
        part = o_scr[2 * h] * coef[:, 2 * h : 2 * h + 1] + o_scr[2 * h + 1] * coef[:, 2 * h + 1 : 2 * h + 2]
        d_out[h] = part.astype(BF16)
    d_all[tp] = d_out[tp]

    @pl.loop(1, TP)
    def _(p):
        peer = wrap(tp + p)
        x_copy(2, d_out.at[peer], d_all, tp, peer).start()

    w.far_steps(2, 3, 8)
    x_wait(2, d_all)
    difference = jnp.sum(d_all[...].astype(F32), axis=0)
    square = jnp.mean(difference * difference, axis=-1, keepdims=True)
    ho_all[tp] = (difference * lax.rsqrt(square + EPSILON) * hgain_ref[...]).astype(BF16)
    w.far_steps(3, 0, 1)
    x_share(3, ho_all)
    w.far_steps(3, 1, 4)
    x_wait(3, ho_all)
    projected = jnp.zeros((ROWS, 256), F32)
    for h in range(HEADS):
        projected += jnp.dot(ho_all[h], ow_ref[h * 256 : (h + 1) * 256], preferred_element_type=F32)
    after_mix = res_ref[...].astype(F32) + projected
    am_scr[...] = after_mix
    an_all[tp] = (after_mix * ngain_ref[...]).astype(BF16)
    squares = jnp.sum(after_mix * after_mix, axis=1, keepdims=True)
    sq_all[tp] = jnp.transpose(jnp.broadcast_to(squares, (ROWS, 128)))[0:8]
    w.far_steps(3, 4, 5)
    x_share(4, an_all)
    x_share(5, sq_all)
    w.far_steps(3, 5, 8)
    x_wait(4, an_all)
    x_wait(5, sq_all)
    squares = jnp.sum(sq_all[...], axis=0)
    squares = jnp.transpose(jnp.broadcast_to(squares[0:1], (128, 128)))[:, 0:1]
    scale = lax.rsqrt(squares / D + EPSILON)
    w.far_steps(4, 0, 8)

    hid_scr[...] = jnp.zeros_like(hid_scr)

    @pl.loop(0, TP)
    def _(t):
        hid_scr[...] += jnp.dot(an_all[t], up_all[pl.ds(t * RING, RING)].reshape(256, 1024), preferred_element_type=F32)

    activated = jnp.square(jax.nn.relu(hid_scr[...] * scale)).astype(BF16)

    def mixed(t):
        return lax.dot_general(activated, dn_all[pl.ds(t * RING, RING)].reshape(256, 1024), NT, preferred_element_type=F32)

    def rs_copy(p):
        peer = wrap(tp + p)
        return x_copy(6, rs_out.at[peer], rs_all, tp, peer)

    for p in range(1, TP):
        peer = wrap(tp + p)
        rs_out[peer] = mixed(peer).astype(BF16)
        if p > 1:
            rs_copy(p - 1).start()
    own = am_scr[...] + mixed(tp)
    rs_copy(TP - 1).start()
    rs_all[tp] = jnp.zeros((ROWS, 256), BF16)
    x_wait(6, rs_all)
    out_ref[...] = (own + jnp.sum(rs_all[...].astype(F32), axis=0)).astype(BF16)

    kv.finish()
    w.finish()
    for k, array in enumerate((q_all, st_all, d_out, ho_all, an_all, sq_all, rs_out)):
        x_sent(k, array)


def on_device(residual, queries, key_proj, value_proj, diff_lambda, head_gain, out_weight, norm_gain, up_weight, down_weight):
    vmem = pl.BlockSpec(memory_space=pltpu.VMEM)
    smem = pl.BlockSpec(memory_space=pltpu.SMEM)
    block = (TP, ROWS, 256)
    dma = pltpu.SemaphoreType.DMA
    return pl.pallas_call(
        kernel,
        out_shape=jax.ShapeDtypeStruct((ROWS, 256), BF16),
        in_specs=[vmem, vmem, vmem, vmem, smem] + [vmem] * 5,
        out_specs=vmem,
        scratch_shapes=[
            pltpu.VMEM((RING * RING, 16, 512), BF16),
            pltpu.VMEM((RING * RING, 16, 512), BF16),
            pltpu.VMEM((RING * RING, 32, 1024), BF16),
            pltpu.VMEM((RING * RING, 32, 1024), BF16),
            pltpu.VMEM(block, BF16),
            pltpu.VMEM((TP, 32, 128), F32),
            pltpu.VMEM(block, BF16),
            pltpu.VMEM(block, BF16),
            pltpu.VMEM(block, BF16),
            pltpu.VMEM(block, BF16),
            pltpu.VMEM((TP, 8, 128), F32),
            pltpu.VMEM(block, BF16),
            pltpu.VMEM(block, BF16),
            pltpu.VMEM((16, ROWS, 256), F32),
            pltpu.VMEM((ROWS, 256), F32),
            pltpu.VMEM((ROWS, 1024), F32),
            dma((2,)), dma((2, 2, 4)), dma((2, 2, 4, 8)),
            dma((2,)), dma((2, 2, 4)), dma((2, 2, 4, 8)),
            dma((7,)), dma((7, TP)),
        ],
        compiler_params=pltpu.CompilerParams(
            collective_id=0, has_side_effects=True, vmem_limit_bytes=48 * 1024 * 1024),
    )(residual, queries, key_proj, value_proj, diff_lambda, head_gain.reshape(1, 256), out_weight,
      norm_gain.reshape(1, 256), up_weight, down_weight)


def solution(mesh):
    return jax.shard_map(
        on_device,
        mesh=mesh,
        in_specs=(
            P("sp", "tp"),
            P("sp", "tp"),
            P(("sp", "tp"), None),
            P(("sp", "tp"), None),
            P(),
            P(),
            P(None, "tp"),
            P("tp"),
            P("sp", "tp"),
            P("tp", "sp"),
        ),
        out_specs=P("sp", "tp"),
        check_vma=False,
    )
```

time: 232 us -> 102 us (0.44)
  waiting for transfers between devices: 114 us -> 0 us
  Pallas kernels: 0 us -> 99 us
  blocking collectives: 53.1 us -> 0 us
  starting transfers between devices: 20.3 us -> 0 us
  between operations: 13.6 us -> 0.13 us
  matrix products: 11.5 us -> 0 us
  other arithmetic: 9.83 us -> 0 us
  local copies, waits for them, and re-layouts: 9.31 us -> 3 us
    pallas_call x0 -> x1, Pallas kernels: none -> 99 us  [on_device(): pl.pallas_call(kernel, out_shape=jax.ShapeDtypeStruct((ROWS, 256), BF16),...]
    all_gather x2 -> x0, waiting for transfers between devices: 87.8 us -> none  [the longest x1 72.8 us: sent_together(): lax.all_gather(both, axis, axis=dim, tiled=True)]
    all_to_all x4 -> x0, blocking collectives: 53.1 us -> none  [the longest x3 33.2 us: from_everyone(): return lax.all_to_all(copies, axis, split_axis=0, concat_axis=0, tiled=True)]
    all_to_all x2 -> x0, waiting for transfers between devices: 25.8 us -> none  [the longest x1 25.8 us: side_by_side(): lax.all_to_all(both, axis, split_axis=split_dim, concat_axis=concat_dim,...]
    all_to_all x2 -> x0, starting transfers between devices: 20.2 us -> none  [the longest x1 10.9 us: from_everyone(): return lax.all_to_all(copies, axis, split_axis=0, concat_axis=0, tiled=True)]
    dot_general x4 -> x0, matrix products: 11.5 us -> none  [the longest x1 5.59 us: on_device(): jnp.dot(activated, down_whole, preferred_element_type=jnp.float32)]
    concatenate x3 -> x0, other arithmetic: 5.07 us -> none  [the longest x1 2.1 us: side_by_side(): both = jnp.concatenate(columns, axis=along)]
    reduce_sum x6 -> x0, other arithmetic: 3.78 us -> none  [the longest x1 1.77 us: on_device(): totals = jnp.sum(weights, axis=-1)]
  transfers between devices with their start and end apart: 4 -> 0, of which waited for: 3 -> 0; matrix products, arithmetic and copies ran while one was open for 10% -> 0% of each run, Pallas kernels for 0% -> 0%
where the time goes in v1:
time: 102 us
  Pallas kernels  99 us (97%)
  local copies, waits for them, and re-layouts  3 us (3%)
    pallas_call x1, Pallas kernels, on_device(): pl.pallas_call(kernel, out_shape=jax.ShapeDtypeStruct((ROWS, 256), BF16),...  99 us
    unnamed x20, local copies, waits for them, and re-layouts  3 us

profile of v1, /device:TPU:1, one launch (start us, length us, event | category | flops | bytes accessed | tf_op | source)
XLA Modules:
  0.0 102.1 jit_solution(13433509208571939230)
XLA Ops:
  0.0 0.0 copy-start.1
  0.0 0.0 copy-start.2
  0.0 0.0 copy-start.3
  0.0 0.0 copy-start.4
  0.0 0.0 copy-start.5
  0.0 0.0 copy-start.6
  0.0 0.0 copy-start.7
  0.0 0.0 copy-start.8
  0.1 1.1 %copy.11.down_ref = bf16[1024,32]{1,0:T(8,128)(2,1)S(1)} copy(bf16[1024,32]{0,1:T(8,128)(2,1)} %param.19) | data formatting | bytes 131072 | tf_op args[9]
  1.2 0.0 copy-done.1
  1.2 0.0 copy-done.2
  1.2 0.0 copy-done.3
  1.2 0.0 copy-done.4
  1.2 0.0 copy-done.5
  1.2 0.0 copy-done.6
  1.2 0.0 copy-done.7
  1.3 0.0 copy-done.8
  1.3 0.0 copy-start
  1.3 1.2 %copy-done = bf16[2048,256]{1,0:T(8,128)(2,1)S(1)} copy-done((bf16[2048,256]{1,0:T(8,128)(2,1)S(1)}, bf16[2048,256]{1,0:T(8,128)(2,1)}, u32[]{:S(2)}) %copy-start) | copy-done | bytes 1048600
  2.5 99.0 %shard_map.100 = bf16[128,256]{1,0:T(8,128)(2,1)S(1)} custom-call(bf16[128,256]{1,0:T(8,128)(2,1)S(1)} %copy-done.1, bf16[128,256]{1,0:T(8,128)(2,1)S(1)} %copy-done.2, bf16[16,512]{1,0:T(8,128)(2,1)S(1)} %copy-done.4, bf16[16,512]{1,0:T(8,128)(2,1)S(1)} %copy-done.5, f32[8]{0:T(128)S(1)} %copy-done.8, f32[1,256]{1,0:T(1,128)S(1)} %bitcast.2, ...), custom_call_target="tpu_custom_call" | custom-call | tf_op jit(solution)/shard_map/pallas_call | solution.py:305
  101.5 0.6 copy.13
Async XLA Ops:
  0.0 1.2 %copy-start.1 = (bf16[128,256]{1,0:T(8,128)(2,1)S(1)}, bf16[128,256]{1,0:T(8,128)(2,1)}, u32[]{:S(2)}) copy-start(bf16[128,256]{1,0:T(8,128)(2,1)} %res_ref.1) | copy-start | bytes 196612
  0.0 1.2 %copy-start.2 = (bf16[128,256]{1,0:T(8,128)(2,1)S(1)}, bf16[128,256]{1,0:T(8,128)(2,1)}, u32[]{:S(2)}) copy-start(bf16[128,256]{1,0:T(8,128)(2,1)} %q_ref.1) | copy-start | bytes 196612
  0.0 1.2 %copy-start.3 = (bf16[32,1024]{1,0:T(8,128)(2,1)S(1)}, bf16[32,1024]{1,0:T(8,128)(2,1)}, u32[]{:S(2)}) copy-start(bf16[32,1024]{1,0:T(8,128)(2,1)} %up_ref.1) | copy-start | bytes 196612
  0.0 1.2 %copy-start.4 = (bf16[16,512]{1,0:T(8,128)(2,1)S(1)}, bf16[16,512]{1,0:T(8,128)(2,1)}, u32[]{:S(2)}) copy-start(bf16[16,512]{1,0:T(8,128)(2,1)} %key_ref.1) | copy-start | bytes 49156
  0.0 1.2 %copy-start.5 = (bf16[16,512]{1,0:T(8,128)(2,1)S(1)}, bf16[16,512]{1,0:T(8,128)(2,1)}, u32[]{:S(2)}) copy-start(bf16[16,512]{1,0:T(8,128)(2,1)} %val_ref.1) | copy-start | bytes 49156
  0.0 1.2 %copy-start.6 = (f32[256]{0:T(256)S(1)}, f32[256]{0:T(256)}, u32[]{:S(2)}) copy-start(f32[256]{0:T(256)} %param.15) | copy-start | bytes 3076
  0.0 1.2 %copy-start.7 = (f32[256]{0:T(256)S(1)}, f32[256]{0:T(256)}, u32[]{:S(2)}) copy-start(f32[256]{0:T(256)} %param.17) | copy-start | bytes 3076
  0.0 1.2 %copy-start.8 = (f32[8]{0:T(128)S(1)}, f32[8]{0:T(128)}, u32[]{:S(2)}) copy-start(f32[8]{0:T(128)} %lam_ref.1) | copy-start | bytes 100
  1.3 1.2 %copy-start = (bf16[2048,256]{1,0:T(8,128)(2,1)S(1)}, bf16[2048,256]{1,0:T(8,128)(2,1)}, u32[]{:S(2)}) copy-start(bf16[2048,256]{1,0:T(8,128)(2,1)} %ow_ref.1) | copy-start | bytes 3145732

commit v2 on v1

v2 whole, which is shorter than its diff:
```python
import jax
import jax.numpy as jnp
from jax import lax
from jax.experimental import pallas as pl
from jax.experimental.pallas import tpu as pltpu
from jax.sharding import PartitionSpec as P

D = 2048
HEADS = 8
HEAD_DIM = 128
VALUE_DIM = 256
RING = 8
TP = 8
ROWS = 128
EPSILON = 1e-06
MESH = pl.DeviceIdType.MESH
F32 = jnp.float32
BF16 = jnp.bfloat16
LOG_SCALE = HEAD_DIM ** (-0.5) * 1.4426950408889634
NT = (((1,), (1,)), ((), ()))


def wrap(i):
    return lax.rem(i + RING, RING)


class Gather:
    def __init__(self, first, second, y, z, tp, send, near, far, direct):
        self.direct = direct
        self.arrays = (first, second)
        self.y, self.z, self.tp = y, z, tp
        self.send, self.near, self.far = send, near, far

    def chunk(self, kind, p2, p1):
        array = self.arrays[kind]
        return array.at[p2 * RING + p1] if kind == 0 else array.at[p1 * RING + p2]

    def me1(self, kind):
        return self.y if kind == 0 else self.z

    def me2(self, kind):
        return self.z if kind == 0 else self.y

    def device(self, along_y, step):
        if along_y:
            return (self.z * RING + wrap(self.y + step), self.tp)
        return (wrap(self.z + step) * RING + self.y, self.tp)

    def near_copy(self, kind, way, s, at):
        c = self.chunk(kind, self.me2(kind), at)
        return pltpu.make_async_remote_copy(
            src_ref=c, dst_ref=c, send_sem=self.send.at[kind],
            recv_sem=self.near.at[kind, way, s],
            device_id=self.device(kind == 0, (1 - 2 * way) * (s + 1 if self.direct else 1)),
            device_id_type=MESH)

    def far_copy(self, kind, way, s, at2, at1):
        c = self.chunk(kind, at2, at1)
        return pltpu.make_async_remote_copy(
            src_ref=c, dst_ref=c, send_sem=self.send.at[kind],
            recv_sem=self.far.at[kind, way, s, at1],
            device_id=self.device(kind == 1, 1 - 2 * way), device_id_type=MESH)

    def open_chunk(self, kind, at1):
        for way in range(2):
            self.far_copy(kind, way, 0, self.me2(kind), at1).start()

    def begin(self):
        for s in range(4 if self.direct else 1):
            for kind in range(2):
                for way in range(2 if s < 3 else 1):
                    self.near_copy(kind, way, s, self.me1(kind)).start()
        for kind in range(2):
            self.open_chunk(kind, self.me1(kind))

    def near_step(self, u):
        for way in range(2):
            if way == 1 and u == 4:
                continue
            for kind in range(2):
                at = wrap(self.me1(kind) - u * (1 - 2 * way))
                self.near_copy(kind, way, u - 1, at).wait_recv()
                if u < 4 - way and not self.direct:
                    self.near_copy(kind, way, u, at).start()
                self.open_chunk(kind, at)

    def far_step(self, s, j):
        half = lax.div(j + 1, 2)
        offset = half * (1 - 2 * lax.rem(j, 2))
        for way in range(2):
            mine = lax.rem(j, 2) == way
            for kind in range(2):
                at1 = wrap(self.me1(kind) + offset)
                at2 = wrap(self.me2(kind) - s * (1 - 2 * way))

                def arrive():
                    self.far_copy(kind, way, s - 1, at2, at1).wait_recv()

                def forward():
                    self.far_copy(kind, way, s, at2, at1).start()

                if s < 4:
                    arrive()
                else:
                    pl.when(mine)(arrive)
                if s < 3:
                    forward()
                elif s == 3:
                    pl.when(mine)(forward)

    def far_steps(self, s, low, high):
        @pl.loop(low, high)
        def _(j):
            self.far_step(s, j)

    def finish(self):
        for kind in range(2):
            part = self.arrays[kind].at[0 : RING * RING - 1]
            pltpu.make_async_remote_copy(
                src_ref=part, dst_ref=part, send_sem=self.send.at[kind],
                recv_sem=self.near.at[kind, 0, 0],
                device_id=self.device(True, 1), device_id_type=MESH).wait_send()


def kernel(
    res_ref, q_ref, key_ref, val_ref, lam_ref, hgain_ref, ow_ref, ngain_ref, up_ref, down_ref,
    out_ref,
    k_all, v_all, up_all, dn_all, q_all, st_all, ho_all, an_all, sq_all,
    pre_out, pre_in, rs_out, rs_all, keep, o_scr, am_scr, hid_scr,
    kv_send, kv_near, kv_far, w_send, w_near, w_far, x_send, x_recv, pre_send, pre_recv,
):
    sp, tp = lax.axis_index("sp"), lax.axis_index("tp")
    z, y = lax.div(sp, RING), lax.rem(sp, RING)
    kv = Gather(k_all, v_all, y, z, tp, kv_send, kv_near, kv_far, True)
    w = Gather(up_all, dn_all, y, z, tp, w_send, w_near, w_far, False)

    barrier = pltpu.get_barrier_semaphore()

    @pl.loop(1, TP)
    def _(p):
        pl.semaphore_signal(barrier, inc=1, device_id=(sp, wrap(tp + p)), device_id_type=MESH)

    @pl.loop(1, RING)
    def _(p):
        for along_y in (True, False):
            pl.semaphore_signal(barrier, inc=1, device_id=kv.device(along_y, p), device_id_type=MESH)

    k_all[sp] = key_ref[...]
    v_all[sp] = val_ref[...]
    up_all[sp] = up_ref[...]
    rows = lax.broadcasted_iota(jnp.int32, (32, 32), 0)
    cols = lax.broadcasted_iota(jnp.int32, (32, 32), 1)
    eye = jnp.where(rows == cols, 1.0, 0.0).astype(BF16)
    dn_all[sp] = lax.dot_general(eye, down_ref[...], NT, preferred_element_type=F32).astype(BF16)
    q_all[tp] = q_ref[...]

    pl.semaphore_wait(barrier, TP - 1 + 2 * (RING - 1))

    x, c = lax.div(tp, 2), lax.rem(tp, 2)

    def chip(step):
        return lax.rem(x + step + 4, 4)

    def tp_of(step):
        return chip(step) * 2 + c

    partner = x * 2 + 1 - c

    def x_copy(k, src, dst, slot, peer):
        return pltpu.make_async_remote_copy(
            src_ref=src, dst_ref=dst.at[slot], send_sem=x_send.at[k], recv_sem=x_recv.at[k, slot],
            device_id=(sp, peer), device_id_type=MESH)

    def x_arrived(k, dst, slot):
        x_copy(k, dst.at[slot], dst, slot, partner).wait_recv()

    def share(k, array):
        for step in (2, 1, 3):
            x_copy(k, array.at[tp], array, tp, tp_of(step)).start()
        x_copy(k, array.at[tp], array, tp, partner).start()

    def relay(k, array):
        for step in (1, 3, 2):
            slot = tp_of(step)
            x_arrived(k, array, slot)
            x_copy(k, array.at[slot], array, slot, partner).start()

    def collect(k, array):
        for step in (0, 1, 3, 2):
            x_arrived(k, array, chip(step) * 2 + 1 - c)

    def x_sent(k, part):
        pltpu.make_async_remote_copy(
            src_ref=part, dst_ref=part, send_sem=x_send.at[k], recv_sem=x_recv.at[k, 0],
            device_id=(sp, partner), device_id_type=MESH).wait_send()

    events = [(s, j) for s in range(1, 5) for j in range(8)]

    def pump(count):
        for _ in range(count):
            s, j = events.pop(0)
            w.far_step(s, j)

    def reduce_pair(k, produce, gone):
        for i in range(4):
            pre_out[k, i] = produce(i, 2 * i + 1 - c).astype(BF16)
        copy = pltpu.make_async_remote_copy(
            src_ref=pre_out.at[k], dst_ref=pre_in.at[k], send_sem=pre_send.at[k], recv_sem=pre_recv.at[k],
            device_id=(sp, partner), device_id_type=MESH)
        copy.start()
        for i in range(4):
            keep[i] = produce(i, 2 * i + c)
        copy.wait_recv()
        for step in (2, 1, 3):
            i = chip(step)
            rs_out[k, i] = (keep[i] + pre_in[k, i].astype(F32)).astype(BF16)
        for step in (2, 1, 3):
            i = chip(step)
            x_copy(gone, rs_out.at[k, i], rs_all.at[k], x, tp_of(step)).start()
        return keep[x] + pre_in[k, x].astype(F32)

    def reduce_rest(k, gone, total):
        for step in (1, 3, 2):
            i = chip(step)
            x_arrived(gone, rs_all.at[k], i)
            total += rs_all[k, i].astype(F32)
        return total

    kv.begin()
    share(0, q_all)
    w.begin()
    for u in range(1, 5):
        kv.near_step(u)
    relay(0, q_all)
    for s in range(1, 4):
        kv.far_steps(s, 0, 8)
        w.near_step(s)
    w.near_step(4)
    kv.far_steps(4, 0, 8)
    collect(0, q_all)

    lane = lax.broadcasted_iota(jnp.int32, (ROWS, 128), 1)
    stats = jnp.zeros((ROWS, 128), F32)
    for gc in range(4):
        g, m_c = gc // 2, gc % 2
        q = q_all[4 * g : 4 * g + 4, :, m_c * 128 : m_c * 128 + 128].reshape(4 * ROWS, 128)
        k = k_all[:, :, gc * 128 : gc * 128 + 128].reshape(1024, 128)
        v = v_all[:, :, g * 256 : g * 256 + 256].reshape(1024, 256)
        s = lax.dot_general(q, k, NT, preferred_element_type=F32)
        m = jnp.max(s, axis=1, keepdims=True)
        p = jnp.exp2((s - m) * LOG_SCALE)
        t = jnp.sum(p, axis=1, keepdims=True)
        o = jnp.dot(p.astype(BF16), v, preferred_element_type=F32)
        m = m * LOG_SCALE
        for i in range(4):
            at = (4 * g + i) * 2 + m_c
            o_scr[at] = o[i * ROWS : (i + 1) * ROWS]
            stats = jnp.where(lane == at, m[i * ROWS : (i + 1) * ROWS], stats)
            stats = jnp.where(lane == at + 16, t[i * ROWS : (i + 1) * ROWS], stats)
        pump(2)

    st_all[tp] = jnp.transpose(stats)[0:32]
    pump(1)
    for step in (2, 1, 3):
        for core in range(2):
            x_copy(1, st_all.at[tp], st_all, tp, chip(step) * 2 + core).start()
    x_copy(1, st_all.at[tp], st_all, tp, partner).start()
    pump(2)
    x_arrived(1, st_all, partner)
    for step in (1, 3, 2):
        for core in range(2):
            x_arrived(1, st_all, chip(step) * 2 + core)

    every = st_all[...]
    maxima, totals = every[:, 0:16], every[:, 16:32]
    highest = jnp.max(maxima, axis=0)
    total = jnp.sum(jnp.exp2(maxima - highest[None]) * totals, axis=0)
    mine = st_all[tp]
    coef = jnp.exp2(mine[0:16] - highest) / total
    row = lax.broadcasted_iota(jnp.int32, (16, 128), 0)
    factor = jnp.ones((16, 128), F32)
    for h in range(HEADS):
        factor = jnp.where(row == 2 * h + 1, -lam_ref[h], factor)
    coef = jnp.concatenate([coef * factor, jnp.zeros((112, 128), F32)], axis=0)
    coef = jnp.transpose(coef)

    def differ(i, h):
        even = lax.rem(h, 2) == 0
        first = jnp.where(even, coef[:, 4 * i : 4 * i + 1], coef[:, 4 * i + 2 : 4 * i + 3])
        second = jnp.where(even, coef[:, 4 * i + 1 : 4 * i + 2], coef[:, 4 * i + 3 : 4 * i + 4])
        return o_scr[2 * h] * first + o_scr[2 * h + 1] * second

    difference = reduce_pair(0, differ, 2)
    pump(4)
    difference = reduce_rest(0, 2, difference)
    square = jnp.mean(difference * difference, axis=-1, keepdims=True)
    ho_all[tp] = (difference * lax.rsqrt(square + EPSILON) * hgain_ref[...]).astype(BF16)
    pump(1)
    share(3, ho_all)
    pump(3)
    relay(3, ho_all)
    pump(2)
    collect(3, ho_all)
    projected = jnp.zeros((ROWS, 256), F32)
    for h in range(HEADS):
        projected += jnp.dot(ho_all[h], ow_ref[h * 256 : (h + 1) * 256], preferred_element_type=F32)
    after_mix = res_ref[...].astype(F32) + projected
    am_scr[...] = after_mix
    an_all[tp] = (after_mix * ngain_ref[...]).astype(BF16)
    squares = jnp.sum(after_mix * after_mix, axis=1, keepdims=True)
    sq_all[tp] = jnp.transpose(jnp.broadcast_to(squares, (ROWS, 128)))[0:8]
    pump(1)
    share(4, an_all)
    share(5, sq_all)
    pump(2)
    relay(4, an_all)
    relay(5, sq_all)
    pump(2)
    collect(4, an_all)
    collect(5, sq_all)
    squares = jnp.sum(sq_all[...], axis=0)
    squares = jnp.transpose(jnp.broadcast_to(squares[0:1], (128, 128)))[:, 0:1]
    scale = lax.rsqrt(squares / D + EPSILON)
    pump(len(events))

    hid_scr[...] = jnp.zeros_like(hid_scr)

    @pl.loop(0, TP)
    def _(t):
        hid_scr[...] += jnp.dot(
            an_all[t], up_all[pl.ds(t * RING, RING)].reshape(256, 1024), preferred_element_type=F32)

    activated = jnp.square(jax.nn.relu(hid_scr[...] * scale)).astype(BF16)

    def mixed(i, t):
        weights = dn_all[pl.ds(t * RING, RING)].reshape(256, 1024)
        return lax.dot_general(activated, weights, NT, preferred_element_type=F32)

    own = reduce_pair(1, mixed, 6) + am_scr[...]
    out_ref[...] = reduce_rest(1, 6, own).astype(BF16)

    kv.finish()
    w.finish()
    for k, array in ((0, q_all), (1, st_all), (3, ho_all), (4, an_all), (5, sq_all)):
        x_sent(k, array.at[0:7])
    for k, gone in ((0, 2), (1, 6)):
        x_sent(gone, rs_out.at[k, 0:3])
        pltpu.make_async_remote_copy(
            src_ref=pre_out.at[k], dst_ref=pre_in.at[k], send_sem=pre_send.at[k], recv_sem=pre_recv.at[k],
            device_id=(sp, partner), device_id_type=MESH).wait_send()


def on_device(residual, queries, key_proj, value_proj, diff_lambda, head_gain, out_weight, norm_gain, up_weight, down_weight):
    vmem = pl.BlockSpec(memory_space=pltpu.VMEM)
    smem = pl.BlockSpec(memory_space=pltpu.SMEM)
    block = (TP, ROWS, 256)
    dma = pltpu.SemaphoreType.DMA
    return pl.pallas_call(
        kernel,
        out_shape=jax.ShapeDtypeStruct((ROWS, 256), BF16),
        in_specs=[vmem, vmem, vmem, vmem, smem] + [vmem] * 5,
        out_specs=vmem,
        scratch_shapes=[
            pltpu.VMEM((RING * RING, 16, 512), BF16),
            pltpu.VMEM((RING * RING, 16, 512), BF16),
            pltpu.VMEM((RING * RING, 32, 1024), BF16),
            pltpu.VMEM((RING * RING, 32, 1024), BF16),
            pltpu.VMEM(block, BF16),
            pltpu.VMEM((TP, 32, 128), F32),
            pltpu.VMEM(block, BF16),
            pltpu.VMEM(block, BF16),
            pltpu.VMEM((TP, 8, 128), F32),
            pltpu.VMEM((2, 4, ROWS, 256), BF16),
            pltpu.VMEM((2, 4, ROWS, 256), BF16),
            pltpu.VMEM((2, 4, ROWS, 256), BF16),
            pltpu.VMEM((2, 4, ROWS, 256), BF16),
            pltpu.VMEM((4, ROWS, 256), F32),
            pltpu.VMEM((16, ROWS, 256), F32),
            pltpu.VMEM((ROWS, 256), F32),
            pltpu.VMEM((ROWS, 1024), F32),
            dma((2,)), dma((2, 2, 4)), dma((2, 2, 4, 8)),
            dma((2,)), dma((2, 2, 4)), dma((2, 2, 4, 8)),
            dma((7,)), dma((7, TP)), dma((2,)), dma((2,)),
        ],
        compiler_params=pltpu.CompilerParams(
            collective_id=0, has_side_effects=True, vmem_limit_bytes=48 * 1024 * 1024),
    )(residual, queries, key_proj, value_proj, diff_lambda, head_gain.reshape(1, 256), out_weight,
      norm_gain.reshape(1, 256), up_weight, down_weight)


def solution(mesh):
    return jax.shard_map(
        on_device,
        mesh=mesh,
        in_specs=(
            P("sp", "tp"),
            P("sp", "tp"),
            P(("sp", "tp"), None),
            P(("sp", "tp"), None),
            P(),
            P(),
            P(None, "tp"),
            P("tp"),
            P("sp", "tp"),
            P("tp", "sp"),
        ),
        out_specs=P("sp", "tp"),
        check_vma=False,
    )
```

time: 102 us -> 93.6 us (0.918)
  Pallas kernels: 99 us -> 90.3 us
    pallas_call x1, Pallas kernels: 99 us -> 90.3 us  [on_device(): pl.pallas_call(kernel, out_shape=jax.ShapeDtypeStruct((ROWS, 256), BF16),...]
where the time goes in v2:
time: 93.6 us; the launch traced here: 93.4 us
  Pallas kernels  90.3 us (96%)
  local copies, waits for them, and re-layouts  3 us (3%)
    pallas_call x1, Pallas kernels, on_device(): pl.pallas_call(kernel, out_shape=jax.ShapeDtypeStruct((ROWS, 256), BF16),...  90.3 us
    unnamed x20, local copies, waits for them, and re-layouts  3 us

profile of v2, /device:TPU:1, one launch (start us, length us, event | category | flops | bytes accessed | tf_op | source)
XLA Modules:
  0.0 93.4 jit_solution(11894795298185809160)
XLA Ops:
  0.0 0.0 copy-start.1
  0.0 0.0 copy-start.2
  0.0 0.0 copy-start.3
  0.0 0.0 copy-start.4
  0.0 0.0 copy-start.5
  0.0 0.0 copy-start.6
  0.0 0.0 copy-start.7
  0.0 0.0 copy-start.8
  0.1 1.1 %copy.11.down_ref = bf16[1024,32]{1,0:T(8,128)(2,1)S(1)} copy(bf16[1024,32]{0,1:T(8,128)(2,1)} %param.19) | data formatting | bytes 131072 | tf_op args[9]
  1.2 0.0 copy-done.1
  1.2 0.0 copy-done.2
  1.2 0.0 copy-done.3
  1.2 0.0 copy-done.4
  1.2 0.0 copy-done.5
  1.2 0.0 copy-done.6
  1.2 0.0 copy-done.7
  1.3 0.0 copy-done.8
  1.3 0.0 copy-start
  1.3 1.2 %copy-done = bf16[2048,256]{1,0:T(8,128)(2,1)S(1)} copy-done((bf16[2048,256]{1,0:T(8,128)(2,1)S(1)}, bf16[2048,256]{1,0:T(8,128)(2,1)}, u32[]{:S(2)}) %copy-start) | copy-done | bytes 1048600
  2.5 90.3 %shard_map.100 = bf16[128,256]{1,0:T(8,128)(2,1)S(1)} custom-call(bf16[128,256]{1,0:T(8,128)(2,1)S(1)} %copy-done.1, bf16[128,256]{1,0:T(8,128)(2,1)S(1)} %copy-done.2, bf16[16,512]{1,0:T(8,128)(2,1)S(1)} %copy-done.4, bf16[16,512]{1,0:T(8,128)(2,1)S(1)} %copy-done.5, f32[8]{0:T(128)S(1)} %copy-done.8, f32[1,256]{1,0:T(1,128)S(1)} %bitcast.2, ...), custom_call_target="tpu_custom_call" | custom-call | tf_op jit(solution)/shard_map/pallas_call | solution.py:358
  92.8 0.6 copy.13
Async XLA Ops:
  0.0 1.2 %copy-start.1 = (bf16[128,256]{1,0:T(8,128)(2,1)S(1)}, bf16[128,256]{1,0:T(8,128)(2,1)}, u32[]{:S(2)}) copy-start(bf16[128,256]{1,0:T(8,128)(2,1)} %res_ref.1) | copy-start | bytes 196612
  0.0 1.2 %copy-start.2 = (bf16[128,256]{1,0:T(8,128)(2,1)S(1)}, bf16[128,256]{1,0:T(8,128)(2,1)}, u32[]{:S(2)}) copy-start(bf16[128,256]{1,0:T(8,128)(2,1)} %q_ref.1) | copy-start | bytes 196612
  0.0 1.2 %copy-start.3 = (bf16[32,1024]{1,0:T(8,128)(2,1)S(1)}, bf16[32,1024]{1,0:T(8,128)(2,1)}, u32[]{:S(2)}) copy-start(bf16[32,1024]{1,0:T(8,128)(2,1)} %up_ref.1) | copy-start | bytes 196612
  0.0 1.2 %copy-start.4 = (bf16[16,512]{1,0:T(8,128)(2,1)S(1)}, bf16[16,512]{1,0:T(8,128)(2,1)}, u32[]{:S(2)}) copy-start(bf16[16,512]{1,0:T(8,128)(2,1)} %key_ref.1) | copy-start | bytes 49156
  0.0 1.2 %copy-start.5 = (bf16[16,512]{1,0:T(8,128)(2,1)S(1)}, bf16[16,512]{1,0:T(8,128)(2,1)}, u32[]{:S(2)}) copy-start(bf16[16,512]{1,0:T(8,128)(2,1)} %val_ref.1) | copy-start | bytes 49156
  0.0 1.2 %copy-start.6 = (f32[256]{0:T(256)S(1)}, f32[256]{0:T(256)}, u32[]{:S(2)}) copy-start(f32[256]{0:T(256)} %param.15) | copy-start | bytes 3076
  0.0 1.2 %copy-start.7 = (f32[256]{0:T(256)S(1)}, f32[256]{0:T(256)}, u32[]{:S(2)}) copy-start(f32[256]{0:T(256)} %param.17) | copy-start | bytes 3076
  0.0 1.2 %copy-start.8 = (f32[8]{0:T(128)S(1)}, f32[8]{0:T(128)}, u32[]{:S(2)}) copy-start(f32[8]{0:T(128)} %lam_ref.1) | copy-start | bytes 100
  1.3 1.2 %copy-start = (bf16[2048,256]{1,0:T(8,128)(2,1)S(1)}, bf16[2048,256]{1,0:T(8,128)(2,1)}, u32[]{:S(2)}) copy-start(bf16[2048,256]{1,0:T(8,128)(2,1)} %ow_ref.1) | copy-start | bytes 3145732

commit v3 on v2

v3 whole, which is shorter than its diff:
```python
import jax
import jax.numpy as jnp
from jax import lax
from jax.experimental import pallas as pl
from jax.experimental.pallas import tpu as pltpu
from jax.sharding import PartitionSpec as P

D = 2048
HEADS = 8
HEAD_DIM = 128
RING = 8
TP = 8
ROWS = 128
EPSILON = 1e-06
MESH = pl.DeviceIdType.MESH
F32 = jnp.float32
BF16 = jnp.bfloat16
LOG_SCALE = HEAD_DIM ** (-0.5) * 1.4426950408889634
NT = (((1,), (1,)), ((), ()))


def wrap(i):
    return lax.rem(i + RING, RING)


class Gather:
    def __init__(self, first, second, y, z, tp, sems, direct, group):
        self.arrays = (first, second)
        self.y, self.z, self.tp = y, z, tp
        self.send, self.near, self.far = sems
        self.direct, self.group = direct, group

    def me1(self, kind):
        return self.y if kind == 0 else self.z

    def me2(self, kind):
        return self.z if kind == 0 else self.y

    def device(self, along_y, step):
        if along_y:
            return (self.z * RING + wrap(self.y + step), self.tp)
        return (wrap(self.z + step) * RING + self.y, self.tp)

    def near_copy(self, kind, way, s, at):
        c = self.arrays[kind].at[self.me2(kind), at]
        step = (1 - 2 * way) * (s + 1 if self.direct else 1)
        return pltpu.make_async_remote_copy(
            src_ref=c, dst_ref=c, send_sem=self.send.at[kind, 0], recv_sem=self.near.at[kind, way, s],
            device_id=self.device(kind == 0, step), device_id_type=MESH)

    def far_copy(self, kind, way, s, at2, at1):
        if self.group == 1:
            c = self.arrays[kind].at[at2, at1]
        else:
            c = self.arrays[kind].at[at2, pl.ds(2 * at1, 2)]
        return pltpu.make_async_remote_copy(
            src_ref=c, dst_ref=c, send_sem=self.send.at[kind, 1], recv_sem=self.far.at[kind, way, s, at1],
            device_id=self.device(kind == 1, 1 - 2 * way), device_id_type=MESH)

    def place(self, kind, j):
        me = self.me1(kind)
        if self.group == 1:
            half = lax.div(j + 1, 2)
            return wrap(me + half * (1 - 2 * lax.rem(j, 2)))
        pair, side = lax.div(me, 2), 1 - 2 * lax.rem(me, 2)
        offset = (0, -side, side, 2)[j]
        return lax.rem(pair + offset + 4, 4)

    def open_chunk(self, j):
        for kind in range(2):
            for way in range(2):
                self.far_copy(kind, way, 0, self.me2(kind), self.place(kind, j)).start()

    def begin(self):
        for s in range(4 if self.direct else 1):
            for kind in range(2):
                for way in range(2 if s < 3 else 1):
                    self.near_copy(kind, way, s, self.me1(kind)).start()
        if self.group == 1:
            self.open_chunk(0)

    def near_step(self, u):
        for way in range(2 if u < 4 else 1):
            for kind in range(2):
                at = wrap(self.me1(kind) - u * (1 - 2 * way))
                self.near_copy(kind, way, u - 1, at).wait_recv()
                if u < 4 - way and not self.direct:
                    self.near_copy(kind, way, u, at).start()
        if self.group == 1:
            self.open_chunk(2 * u - 1)
            if u < 4:
                self.open_chunk(2 * u)
        else:
            self.open_chunk(u - 1)

    def far_step(self, s, j):
        for way in range(2):
            mine = lax.rem(jnp.int32(j), 2) == way
            for kind in range(2):
                at1 = self.place(kind, j)
                at2 = wrap(self.me2(kind) - s * (1 - 2 * way))

                def arrive():
                    self.far_copy(kind, way, s - 1, at2, at1).wait_recv()

                def forward():
                    self.far_copy(kind, way, s, at2, at1).start()

                if isinstance(j, int):
                    if s < 4 or j % 2 == way:
                        arrive()
                    if s < 3 or (s == 3 and j % 2 == way):
                        forward()
                    continue
                if s < 4:
                    arrive()
                else:
                    pl.when(mine)(arrive)
                if s < 3:
                    forward()
                elif s == 3:
                    pl.when(mine)(forward)

    def far_steps(self, s):
        @pl.loop(0, 8 // self.group)
        def _(j):
            self.far_step(s, j)

    def finish(self):
        for kind in range(2):
            for i, part in enumerate((self.arrays[kind].at[0, 0:7], self.arrays[kind].at[0:7])):
                pltpu.make_async_remote_copy(
                    src_ref=part, dst_ref=part, send_sem=self.send.at[kind, i],
                    recv_sem=self.near.at[kind, 0, 0],
                    device_id=self.device(True, 1), device_id_type=MESH).wait_send()


def kernel(
    lam_ref, hgain_ref, ngain_ref, res_hbm, q_hbm, key_hbm, val_hbm, ow_hbm, up_hbm, down_hbm,
    out_ref,
    kv_a, kv_b, up_a, up_b, dn_a, dn_b, res_ref, ow_ref, q_all, st_all, ho_all, an_all, sq_all,
    pre_out, pre_in, rs_out, rs_all, keep, o_scr, mix_a, mix_b, got_a, got_b,
    kv_send, kv_near, kv_far, u_send, u_near, u_far, d_send, d_near, d_far,
    x_send, x_recv, pre_send, pre_recv, in_sem,
):
    sp, tp = lax.axis_index("sp"), lax.axis_index("tp")
    z, y = lax.div(sp, RING), lax.rem(sp, RING)
    x, c = lax.div(tp, 2), lax.rem(tp, 2)
    partner = x * 2 + 1 - c
    kv = Gather(kv_a, kv_b, y, z, tp, (kv_send, kv_near, kv_far), True, 1)
    w1 = Gather(up_a, up_b, y, z, tp, (u_send, u_near, u_far), False, 2)
    w2 = Gather(dn_a, dn_b, y, z, tp, (d_send, d_near, d_far), False, 2)

    barrier = pltpu.get_barrier_semaphore()

    @pl.loop(1, RING)
    def _(p):
        pl.semaphore_signal(barrier, inc=1, device_id=(sp, wrap(tp + p)), device_id_type=MESH)
        for along_y in (True, False):
            pl.semaphore_signal(barrier, inc=1, device_id=kv.device(along_y, p), device_id_type=MESH)

    loads = [
        pltpu.make_async_copy(src, dst, in_sem.at[i])
        for i, (src, dst) in enumerate((
            (key_hbm.at[:, 0:256], kv_a.at[z, y, :, 0:256]),
            (val_hbm.at[:, 0:256], kv_a.at[z, y, :, 256:512]),
            (key_hbm.at[:, 256:512], kv_b.at[y, z, :, 0:256]),
            (val_hbm.at[:, 256:512], kv_b.at[y, z, :, 256:512]),
            (q_hbm, q_all.at[tp]),
            (up_hbm.at[:, 0:512], up_a.at[z, y]),
            (up_hbm.at[:, 512:1024], up_b.at[y, z]),
            (down_hbm.at[0:16], dn_a.at[z, y]),
            (down_hbm.at[16:32], dn_b.at[y, z]),
            (res_hbm, res_ref),
            (ow_hbm, ow_ref),
        ))
    ]
    for load in loads:
        load.start()
    for load in loads:
        load.wait()
    pl.semaphore_wait(barrier, TP - 1 + 2 * (RING - 1))

    def chip(step):
        return lax.rem(x + step + 4, 4)

    def tp_of(step):
        return chip(step) * 2 + c

    def x_copy(k, src, dst, slot, peer):
        return pltpu.make_async_remote_copy(
            src_ref=src, dst_ref=dst.at[slot], send_sem=x_send.at[k], recv_sem=x_recv.at[k, slot],
            device_id=(sp, peer), device_id_type=MESH)

    def x_arrived(k, dst, slot):
        x_copy(k, dst.at[slot], dst, slot, partner).wait_recv()

    def share(k, array):
        for step in (2, 1, 3):
            x_copy(k, array.at[tp], array, tp, tp_of(step)).start()
        x_copy(k, array.at[tp], array, tp, partner).start()

    def relay(k, array):
        for step in (1, 3, 2):
            slot = tp_of(step)
            x_arrived(k, array, slot)
            x_copy(k, array.at[slot], array, slot, partner).start()

    def collect(k, array):
        for step in (0, 1, 3, 2):
            x_arrived(k, array, chip(step) * 2 + 1 - c)

    def x_sent(k, part):
        pltpu.make_async_remote_copy(
            src_ref=part, dst_ref=part, send_sem=x_send.at[k], recv_sem=x_recv.at[k, 0],
            device_id=(sp, partner), device_id_type=MESH).wait_send()

    events = [(w1, 1, j) for j in range(4)]
    for j in range(4):
        events += [(w2, 0, j + 1), (w1, 2, j)]
    for j in range(4):
        events += [(w1, 3, j), (w2, 1, j)]
    for j in range(4):
        events += [(w1, 4, j), (w2, 2, j)]

    def pump(count):
        for _ in range(count):
            gather, s, j = events.pop(0)
            if s == 0:
                gather.near_step(j)
            else:
                gather.far_step(s, j)

    kv.begin()
    share(0, q_all)
    w1.begin()
    for u in range(1, 5):
        kv.near_step(u)
    relay(0, q_all)
    for s in range(1, 4):
        kv.far_steps(s)
        w1.near_step(s)
    w1.near_step(4)
    w2.begin()
    kv.far_steps(4)
    collect(0, q_all)

    lane = lax.broadcasted_iota(jnp.int32, (ROWS, 128), 1)
    stats = jnp.zeros((ROWS, 128), F32)
    for gc in range(4):
        g, m_c = gc // 2, gc % 2
        whole = kv_a if g == 0 else kv_b
        q = q_all[4 * g : 4 * g + 4, :, m_c * 128 : m_c * 128 + 128].reshape(4 * ROWS, 128)
        k = whole[:, :, :, m_c * 128 : m_c * 128 + 128].reshape(1024, 128)
        v = whole[:, :, :, 256:512].reshape(1024, 256)
        s = lax.dot_general(q, k, NT, preferred_element_type=F32)
        m = jnp.max(s, axis=1, keepdims=True)
        p = jnp.exp2((s - m) * LOG_SCALE)
        t = jnp.sum(p, axis=1, keepdims=True)
        o = jnp.dot(p.astype(BF16), v, preferred_element_type=F32)
        m = m * LOG_SCALE
        for i in range(4):
            at = (4 * g + i) * 2 + m_c
            o_scr[at] = o[i * ROWS : (i + 1) * ROWS]
            stats = jnp.where(lane == at, m[i * ROWS : (i + 1) * ROWS], stats)
            stats = jnp.where(lane == at + 16, t[i * ROWS : (i + 1) * ROWS], stats)
        pump(1)

    st_all[tp] = jnp.transpose(stats)[0:32]
    pump(1)
    for step in (2, 1, 3):
        for core in range(2):
            x_copy(1, st_all.at[tp], st_all, tp, chip(step) * 2 + core).start()
    x_copy(1, st_all.at[tp], st_all, tp, partner).start()
    pump(2)
    x_arrived(1, st_all, partner)
    for step in (1, 3, 2):
        for core in range(2):
            x_arrived(1, st_all, chip(step) * 2 + core)

    every = st_all[...]
    maxima, totals = every[:, 0:16], every[:, 16:32]
    highest = jnp.max(maxima, axis=0)
    total = jnp.sum(jnp.exp2(maxima - highest[None]) * totals, axis=0)
    mine = st_all[tp]
    coef = jnp.exp2(mine[0:16] - highest) / total
    row = lax.broadcasted_iota(jnp.int32, (16, 128), 0)
    factor = jnp.ones((16, 128), F32)
    for h in range(HEADS):
        factor = jnp.where(row == 2 * h + 1, -lam_ref[h], factor)
    coef = jnp.concatenate([coef * factor, jnp.zeros((112, 128), F32)], axis=0)
    coef = jnp.transpose(coef)

    def differ(i, h):
        even = lax.rem(h, 2) == 0
        first = jnp.where(even, coef[:, 4 * i : 4 * i + 1], coef[:, 4 * i + 2 : 4 * i + 3])
        second = jnp.where(even, coef[:, 4 * i + 1 : 4 * i + 2], coef[:, 4 * i + 3 : 4 * i + 4])
        return o_scr[2 * h] * first + o_scr[2 * h + 1] * second

    for i in range(4):
        pre_out[i] = differ(i, 2 * i + 1 - c).astype(BF16)
    across = pltpu.make_async_remote_copy(
        src_ref=pre_out, dst_ref=pre_in, send_sem=pre_send, recv_sem=pre_recv,
        device_id=(sp, partner), device_id_type=MESH)
    across.start()
    for i in range(4):
        keep[i] = differ(i, 2 * i + c)
    across.wait_recv()
    for step in (2, 1, 3):
        i = chip(step)
        rs_out[i] = (keep[i] + pre_in[i].astype(F32)).astype(BF16)
    for step in (2, 1, 3):
        i = chip(step)
        x_copy(2, rs_out.at[i], rs_all, x, tp_of(step)).start()
    difference = keep[x] + pre_in[x].astype(F32)
    pump(5)
    for step in (1, 3, 2):
        i = chip(step)
        x_arrived(2, rs_all, i)
        difference += rs_all[i].astype(F32)

    square = jnp.mean(difference * difference, axis=-1, keepdims=True)
    ho_all[tp] = (difference * lax.rsqrt(square + EPSILON) * hgain_ref[...]).astype(BF16)
    pump(1)
    share(3, ho_all)
    pump(4)
    relay(3, ho_all)
    pump(1)
    collect(3, ho_all)
    heads = jnp.concatenate([ho_all[h] for h in range(HEADS)], axis=1)
    projected = jnp.dot(heads, ow_ref[...], preferred_element_type=F32)
    after_mix = res_ref[...].astype(F32) + projected
    keep[0] = after_mix
    an_all[tp] = (after_mix * ngain_ref[...]).astype(BF16)
    squares = jnp.sum(after_mix * after_mix, axis=1, keepdims=True)
    sq_all[tp] = jnp.transpose(jnp.broadcast_to(squares, (ROWS, 128)))[0:8]
    pump(1)
    share(4, an_all)
    share(5, sq_all)
    pump(4)
    relay(4, an_all)
    relay(5, sq_all)
    pump(1)
    collect(4, an_all)
    collect(5, sq_all)
    squares = jnp.sum(sq_all[...], axis=0)
    squares = jnp.transpose(jnp.broadcast_to(squares[0:1], (128, 128)))[:, 0:1]
    scale = lax.rsqrt(squares / D + EPSILON)
    pump(len(events))

    normed = jnp.concatenate([an_all[t] for t in range(TP)], axis=1)
    parts = []
    for half in range(2):
        if half == 0:
            weights = up_a[...].reshape(2048, 512)
        else:
            weights = jnp.concatenate([up_b[:, t].reshape(256, 512) for t in range(TP)], axis=0)
        hidden = jnp.dot(normed, weights, preferred_element_type=F32) * scale
        parts.append(jnp.square(jax.nn.relu(hidden)).astype(BF16))
    activated = jnp.concatenate(parts, axis=1)

    def mix(weights):
        return lax.dot_general(
            activated, weights.reshape(128, 1024), NT, preferred_element_type=F32).astype(BF16)

    def give(k, out, got, t):
        @pl.when(t != tp)
        def _():
            x_copy(k, out.at[t], got, tp, t).start()

        @pl.when(t == tp)
        def _():
            got[tp] = out[tp]

    def give_a(places):
        for t in places:
            mix_a[t] = mix(dn_a[t])
        for t in places:
            give(6, mix_a, got_a, t)

    give_a([z])
    give_a([wrap(z + 1), wrap(z - 1)])
    give_a([wrap(z + 2), wrap(z - 2)])
    for j in range(4):
        w2.far_step(3, j)
    give_a([wrap(z + 3), wrap(z - 3)])
    for j in range(4):
        w2.far_step(4, j)

    order = [chip(step) * 2 + core for step in (2, 1, 3, 0) for core in range(2)]
    for n, t in enumerate(order):
        mix_b[t] = mix(dn_b[:, t])
        if n > 0:
            give(7, mix_b, got_b, order[n - 1])
    give(7, mix_b, got_b, order[-1])
    give_a([wrap(z + 4)])

    def spread(got, shift):
        source = lax.broadcasted_iota(jnp.int32, (128, 256), 0)
        target = lax.broadcasted_iota(jnp.int32, (128, 256), 1)
        at = lax.div(source, 16) * 32 + lax.rem(source, 16) + shift
        matrix = jnp.where(at == target, 1.0, 0.0).astype(BF16)
        rows = jnp.concatenate([got[t] for t in range(TP)], axis=1)
        return jnp.dot(rows, jnp.concatenate([matrix] * TP, axis=0), preferred_element_type=F32)

    for k, got in ((6, got_a), (7, got_b)):
        @pl.loop(1, TP)
        def _(p):
            x_arrived(k, got, wrap(tp - p))

    out_ref[...] = (keep[0] + (spread(got_a, 0) + spread(got_b, 16))).astype(BF16)

    kv.finish()
    w1.finish()
    w2.finish()
    for k, array in ((0, q_all), (1, st_all), (3, ho_all), (4, an_all), (5, sq_all), (6, mix_a), (7, mix_b)):
        x_sent(k, array.at[0:7])
    x_sent(2, rs_out.at[0:3])
    across.wait_send()


def on_device(residual, queries, key_proj, value_proj, diff_lambda, head_gain, out_weight, norm_gain, up_weight, down_weight):
    vmem = pl.BlockSpec(memory_space=pltpu.VMEM)
    smem = pl.BlockSpec(memory_space=pltpu.SMEM)
    hbm = pl.BlockSpec(memory_space=pltpu.HBM)
    block = (TP, ROWS, 256)
    half = (TP, ROWS, 128)
    dma = pltpu.SemaphoreType.DMA
    return pl.pallas_call(
        kernel,
        out_shape=jax.ShapeDtypeStruct((ROWS, 256), BF16),
        in_specs=[smem, vmem, vmem] + [hbm] * 7,
        out_specs=vmem,
        scratch_shapes=[
            pltpu.VMEM((RING, RING, 16, 512), BF16),
            pltpu.VMEM((RING, RING, 16, 512), BF16),
            pltpu.VMEM((RING, RING, 32, 512), BF16),
            pltpu.VMEM((RING, RING, 32, 512), BF16),
            pltpu.VMEM((RING, RING, 16, 1024), BF16),
            pltpu.VMEM((RING, RING, 16, 1024), BF16),
            pltpu.VMEM((ROWS, 256), BF16),
            pltpu.VMEM((2048, 256), BF16),
            pltpu.VMEM(block, BF16),
            pltpu.VMEM((TP, 32, 128), F32),
            pltpu.VMEM(block, BF16),
            pltpu.VMEM(block, BF16),
            pltpu.VMEM((TP, 8, 128), F32),
            pltpu.VMEM((4, ROWS, 256), BF16),
            pltpu.VMEM((4, ROWS, 256), BF16),
            pltpu.VMEM((4, ROWS, 256), BF16),
            pltpu.VMEM((4, ROWS, 256), BF16),
            pltpu.VMEM((4, ROWS, 256), F32),
            pltpu.VMEM((16, ROWS, 256), F32),
            pltpu.VMEM(half, BF16),
            pltpu.VMEM(half, BF16),
            pltpu.VMEM(half, BF16),
            pltpu.VMEM(half, BF16),
            dma((2, 2)), dma((2, 2, 4)), dma((2, 2, 4, 8)),
            dma((2, 2)), dma((2, 2, 4)), dma((2, 2, 4, 4)),
            dma((2, 2)), dma((2, 2, 4)), dma((2, 2, 4, 4)),
            dma((8,)), dma((8, TP)), dma, dma, dma((11,)),
        ],
        compiler_params=pltpu.CompilerParams(
            collective_id=0, has_side_effects=True, vmem_limit_bytes=67043328),
    )(diff_lambda, head_gain.reshape(1, 256), norm_gain.reshape(1, 256), residual, queries, key_proj, value_proj,
      out_weight, up_weight, down_weight.T)


def solution(mesh):
    return jax.shard_map(
        on_device,
        mesh=mesh,
        in_specs=(
            P("sp", "tp"),
            P("sp", "tp"),
            P(("sp", "tp"), None),
            P(("sp", "tp"), None),
            P(),
            P(),
            P(None, "tp"),
            P("tp"),
            P("sp", "tp"),
            P("tp", "sp"),
        ),
        out_specs=P("sp", "tp"),
        check_vma=False,
    )
```

time: 93.6 us -> 90.8 us (0.970)
  local copies, waits for them, and re-layouts: 3 us -> 1.47 us
  Pallas kernels: 90.3 us -> 89.1 us
    unnamed x20 -> x1, local copies, waits for them, and re-layouts: 3 us -> 1.47 us
    pallas_call x1, Pallas kernels: 90.3 us -> 89.1 us  [on_device(): pl.pallas_call(kernel, out_shape=jax.ShapeDtypeStruct((ROWS, 256), BF16),...]
where the time goes in v3:
time: 90.8 us; the launch traced here: 90.6 us
  Pallas kernels  89.1 us (98%)
  local copies, waits for them, and re-layouts  1.47 us (2%)
    pallas_call x1, Pallas kernels, on_device(): pl.pallas_call(kernel, out_shape=jax.ShapeDtypeStruct((ROWS, 256), BF16),...  89.1 us

profile of v3, /device:TPU:1, one launch (start us, length us, event | category | flops | bytes accessed | tf_op | source)
XLA Modules:
  0.0 90.6 jit_solution(16294485932288376695)
XLA Ops:
  0.0 89.1 %shard_map.100 = bf16[128,256]{1,0:T(8,128)(2,1)} custom-call(f32[8]{0:T(128)} %lam_ref.1, f32[1,256]{1,0:T(1,128)} %bitcast.4, f32[1,256]{1,0:T(1,128)} %bitcast.5, bf16[128,256]{1,0:T(8,128)(2,1)} %res_hbm.1, bf16[128,256]{1,0:T(8,128)(2,1)} %q_hbm.1, bf16[16,512]{1,0:T(8,128)(2,1)} %key_hbm.1, bf16[16,512]{1,0:T(8,128)(2,1)} %val_hbm.1, ...), custom_call_target="tpu_custom_call" | custom-call | tf_op jit(solution)/shard_map/pallas_call | solution.py:429
  89.1 1.5 %copy.12 = bf16[128,256]{1,0:T(8,128)(2,1)} copy(bf16[128,256]{1,0:T(8,128)(2,1)} %shard_map.100) | data formatting | bytes 131072

commit v4 on v3

--- a/solution.py
+++ b/solution.py
@@ -24,11 +24,11 @@
 
 
 class Gather:
-    def __init__(self, first, second, y, z, tp, sems, direct, group):
+    def __init__(self, first, second, y, z, tp, sems, direct):
         self.arrays = (first, second)
         self.y, self.z, self.tp = y, z, tp
         self.send, self.near, self.far = sems
-        self.direct, self.group = direct, group
+        self.direct = direct
 
     def me1(self, kind):
         return self.y if kind == 0 else self.z
@@ -49,19 +49,13 @@
             device_id=self.device(kind == 0, step), device_id_type=MESH)
 
     def far_copy(self, kind, way, s, at2, at1):
-        if self.group == 1:
-            c = self.arrays[kind].at[at2, at1]
-        else:
-            c = self.arrays[kind].at[at2, pl.ds(2 * at1, 2)]
+        c = self.arrays[kind].at[at2, pl.ds(2 * at1, 2)]
         return pltpu.make_async_remote_copy(
             src_ref=c, dst_ref=c, send_sem=self.send.at[kind, 1], recv_sem=self.far.at[kind, way, s, at1],
             device_id=self.device(kind == 1, 1 - 2 * way), device_id_type=MESH)
 
     def place(self, kind, j):
         me = self.me1(kind)
-        if self.group == 1:
-            half = lax.div(j + 1, 2)
-            return wrap(me + half * (1 - 2 * lax.rem(j, 2)))
         pair, side = lax.div(me, 2), 1 - 2 * lax.rem(me, 2)
         offset = (0, -side, side, 2)[j]
         return lax.rem(pair + offset + 4, 4)
@@ -76,8 +70,6 @@
             for kind in range(2):
                 for way in range(2 if s < 3 else 1):
                     self.near_copy(kind, way, s, self.me1(kind)).start()
-        if self.group == 1:
-            self.open_chunk(0)
 
     def near_step(self, u):
         for way in range(2 if u < 4 else 1):
@@ -86,44 +78,20 @@
                 self.near_copy(kind, way, u - 1, at).wait_recv()
                 if u < 4 - way and not self.direct:
                     self.near_copy(kind, way, u, at).start()
-        if self.group == 1:
-            self.open_chunk(2 * u - 1)
-            if u < 4:
-                self.open_chunk(2 * u)
-        else:
-            self.open_chunk(u - 1)
+        self.open_chunk(u - 1)
 
     def far_step(self, s, j):
         for way in range(2):
-            mine = lax.rem(jnp.int32(j), 2) == way
             for kind in range(2):
                 at1 = self.place(kind, j)
                 at2 = wrap(self.me2(kind) - s * (1 - 2 * way))
-
-                def arrive():
+                if s < 4 or j % 2 == way:
                     self.far_copy(kind, way, s - 1, at2, at1).wait_recv()
-
-                def forward():
+                if s < 3 or (s == 3 and j % 2 == way):
                     self.far_copy(kind, way, s, at2, at1).start()
 
-                if isinstance(j, int):
-                    if s < 4 or j % 2 == way:
-                        arrive()
-                    if s < 3 or (s == 3 and j % 2 == way):
-                        forward()
-                    continue
-                if s < 4:
-                    arrive()
-                else:
-                    pl.when(mine)(arrive)
-                if s < 3:
-                    forward()
-                elif s == 3:
-                    pl.when(mine)(forward)
-
     def far_steps(self, s):
-        @pl.loop(0, 8 // self.group)
-        def _(j):
+        for j in range(4):
             self.far_step(s, j)
 
     def finish(self):
@@ -147,9 +115,9 @@
     z, y = lax.div(sp, RING), lax.rem(sp, RING)
     x, c = lax.div(tp, 2), lax.rem(tp, 2)
     partner = x * 2 + 1 - c
-    kv = Gather(kv_a, kv_b, y, z, tp, (kv_send, kv_near, kv_far), True, 1)
-    w1 = Gather(up_a, up_b, y, z, tp, (u_send, u_near, u_far), False, 2)
-    w2 = Gather(dn_a, dn_b, y, z, tp, (d_send, d_near, d_far), False, 2)
+    kv = Gather(kv_a, kv_b, y, z, tp, (kv_send, kv_near, kv_far), True)
+    w1 = Gather(up_a, up_b, y, z, tp, (u_send, u_near, u_far), False)
+    w2 = Gather(dn_a, dn_b, y, z, tp, (d_send, d_near, d_far), False)
 
     barrier = pltpu.get_barrier_semaphore()
 
@@ -272,7 +240,7 @@
         for core in range(2):
             x_copy(1, st_all.at[tp], st_all, tp, chip(step) * 2 + core).start()
     x_copy(1, st_all.at[tp], st_all, tp, partner).start()
-    pump(2)
+    pump(3)
     x_arrived(1, st_all, partner)
     for step in (1, 3, 2):
         for core in range(2):
@@ -303,8 +271,10 @@
         src_ref=pre_out, dst_ref=pre_in, send_sem=pre_send, recv_sem=pre_recv,
         device_id=(sp, partner), device_id_type=MESH)
     across.start()
+    pump(1)
     for i in range(4):
         keep[i] = differ(i, 2 * i + c)
+    pump(1)
     across.wait_recv()
     for step in (2, 1, 3):
         i = chip(step)
@@ -323,7 +293,7 @@
     ho_all[tp] = (difference * lax.rsqrt(square + EPSILON) * hgain_ref[...]).astype(BF16)
     pump(1)
     share(3, ho_all)
-    pump(4)
+    pump(3)
     relay(3, ho_all)
     pump(1)
     collect(3, ho_all)
@@ -378,44 +348,85 @@
         for t in places:
             give(6, mix_a, got_a, t)
 
+    def mix_block(d):
+        block = dn_b[wrap(y + offsets[d])].reshape(128, 1024)
+        sums = lax.dot_general(block, activated, NT, preferred_element_type=F32)
+        mix_b[:, d] = sums.astype(BF16).reshape(TP, 16, 128)
+
+    def b_copy(k, t, part):
+        return pltpu.make_async_remote_copy(
+            src_ref=mix_b.at[t, part], dst_ref=got_b.at[tp, part], send_sem=x_send.at[k],
+            recv_sem=x_recv.at[k, tp], device_id=(sp, t), device_id_type=MESH)
+
+    def give_b(k, part):
+        for step in (2, 1, 3):
+            for core in range(2):
+                b_copy(k, chip(step) * 2 + core, part).start()
+        b_copy(k, partner, part).start()
+
+    def got_part(k, part):
+        @pl.loop(1, TP)
+        def _(p):
+            slot = wrap(tp - p)
+            there = got_b.at[slot, part]
+            pltpu.make_async_remote_copy(
+                src_ref=there, dst_ref=there, send_sem=x_send.at[k], recv_sem=x_recv.at[k, slot],
+                device_id=(sp, partner), device_id_type=MESH).wait_recv()
+
+    offsets = (0, 1, -1, 2, -2, 3, -3, 4)
+    early, late = pl.ds(0, 7), pl.ds(7, 1)
     give_a([z])
     give_a([wrap(z + 1), wrap(z - 1)])
+    for d in range(3):
+        mix_block(d)
     give_a([wrap(z + 2), wrap(z - 2)])
+    for d in range(3, 5):
+        mix_block(d)
     for j in range(4):
         w2.far_step(3, j)
     give_a([wrap(z + 3), wrap(z - 3)])
+    for d in range(5, 7):
+        mix_block(d)
+    give_b(7, early)
     for j in range(4):
         w2.far_step(4, j)
-
-    order = [chip(step) * 2 + core for step in (2, 1, 3, 0) for core in range(2)]
-    for n, t in enumerate(order):
-        mix_b[t] = mix(dn_b[:, t])
-        if n > 0:
-            give(7, mix_b, got_b, order[n - 1])
-    give(7, mix_b, got_b, order[-1])
+    mix_block(7)
     give_a([wrap(z + 4)])
-
-    def spread(got, shift):
-        source = lax.broadcasted_iota(jnp.int32, (128, 256), 0)
-        target = lax.broadcasted_iota(jnp.int32, (128, 256), 1)
-        at = lax.div(source, 16) * 32 + lax.rem(source, 16) + shift
-        matrix = jnp.where(at == target, 1.0, 0.0).astype(BF16)
-        rows = jnp.concatenate([got[t] for t in range(TP)], axis=1)
-        return jnp.dot(rows, jnp.concatenate([matrix] * TP, axis=0), preferred_element_type=F32)
-
-    for k, got in ((6, got_a), (7, got_b)):
-        @pl.loop(1, TP)
-        def _(p):
-            x_arrived(k, got, wrap(tp - p))
-
-    out_ref[...] = (keep[0] + (spread(got_a, 0) + spread(got_b, 16))).astype(BF16)
+    give_b(8, late)
+    got_b[tp] = mix_b[tp]
+
+    @pl.loop(1, TP)
+    def _(p):
+        x_arrived(6, got_a, wrap(tp - p))
+
+    source = lax.broadcasted_iota(jnp.int32, (128, 256), 0)
+    target = lax.broadcasted_iota(jnp.int32, (128, 256), 1)
+    at = lax.div(source, 16) * 32 + lax.rem(source, 16)
+    spread = jnp.where(at == target, 1.0, 0.0).astype(BF16)
+    rows = jnp.concatenate([got_a[t] for t in range(TP)], axis=1)
+    total = jnp.dot(rows, jnp.concatenate([spread] * TP, axis=0), preferred_element_type=F32)
+    keep[0] = keep[0] + total
+
+    target = lax.broadcasted_iota(jnp.int32, (256, 128), 0)
+    source = lax.broadcasted_iota(jnp.int32, (256, 128), 1)
+    d = lax.div(source, 16)
+    at = y + lax.div(d + 1, 2) * (2 * lax.rem(d, 2) - 1)
+    at = lax.rem(at + RING, RING) * 32 + 16 + lax.rem(source, 16)
+    spread = jnp.where(at == target, 1.0, 0.0).astype(BF16)
+    got_part(7, early)
+    got_part(8, late)
+    total = jnp.dot(
+        jnp.concatenate([spread] * TP, axis=1), got_b[...].reshape(TP * 128, 128), preferred_element_type=F32)
+    out_ref[...] = (keep[0] + jnp.transpose(total)).astype(BF16)
 
     kv.finish()
     w1.finish()
     w2.finish()
-    for k, array in ((0, q_all), (1, st_all), (3, ho_all), (4, an_all), (5, sq_all), (6, mix_a), (7, mix_b)):
+    for k, array in ((0, q_all), (1, st_all), (3, ho_all), (4, an_all), (5, sq_all), (6, mix_a)):
         x_sent(k, array.at[0:7])
     x_sent(2, rs_out.at[0:3])
+    x_sent(7, mix_b.at[0:7, 0:7])
+    x_sent(8, mix_b.at[0, 0:7])
     across.wait_send()
 
 
@@ -452,13 +463,13 @@
             pltpu.VMEM((4, ROWS, 256), F32),
             pltpu.VMEM((16, ROWS, 256), F32),
             pltpu.VMEM(half, BF16),
+            pltpu.VMEM((TP, 8, 16, 128), BF16),
             pltpu.VMEM(half, BF16),
-            pltpu.VMEM(half, BF16),
-            pltpu.VMEM(half, BF16),
-            dma((2, 2)), dma((2, 2, 4)), dma((2, 2, 4, 8)),
+            pltpu.VMEM((TP, 8, 16, 128), BF16),
             dma((2, 2)), dma((2, 2, 4)), dma((2, 2, 4, 4)),
             dma((2, 2)), dma((2, 2, 4)), dma((2, 2, 4, 4)),
-            dma((8,)), dma((8, TP)), dma, dma, dma((11,)),
+            dma((2, 2)), dma((2, 2, 4)), dma((2, 2, 4, 4)),
+            dma((9,)), dma((9, TP)), dma, dma, dma((11,)),
         ],
         compiler_params=pltpu.CompilerParams(
             collective_id=0, has_side_effects=True, vmem_limit_bytes=67043328),

time: 90.8 us -> 89.3 us (0.983)
  Pallas kernels: 89.1 us -> 87.6 us
    pallas_call x1, Pallas kernels: 89.1 us -> 87.6 us  [on_device(): pl.pallas_call(kernel, out_shape=jax.ShapeDtypeStruct((ROWS, 256), BF16),...]
where the time goes in v4:
time: 89.3 us; the launch traced here: 89.1 us
  Pallas kernels  87.6 us (98%)
  local copies, waits for them, and re-layouts  1.47 us (2%)
    pallas_call x1, Pallas kernels, on_device(): pl.pallas_call(kernel, out_shape=jax.ShapeDtypeStruct((ROWS, 256), BF16),...  87.6 us

profile of v4, /device:TPU:1, one launch (start us, length us, event | category | flops | bytes accessed | tf_op | source)
XLA Modules:
  0.0 89.1 jit_solution(9532833560369321404)
XLA Ops:
  0.0 87.6 %shard_map.100 = bf16[128,256]{1,0:T(8,128)(2,1)} custom-call(f32[8]{0:T(128)} %lam_ref.1, f32[1,256]{1,0:T(1,128)} %bitcast.4, f32[1,256]{1,0:T(1,128)} %bitcast.5, bf16[128,256]{1,0:T(8,128)(2,1)} %res_hbm.1, bf16[128,256]{1,0:T(8,128)(2,1)} %q_hbm.1, bf16[16,512]{1,0:T(8,128)(2,1)} %key_hbm.1, bf16[16,512]{1,0:T(8,128)(2,1)} %val_hbm.1, ...), custom_call_target="tpu_custom_call" | custom-call | tf_op jit(solution)/shard_map/pallas_call | solution.py:440
  87.6 1.5 %copy.12 = bf16[128,256]{1,0:T(8,128)(2,1)} copy(bf16[128,256]{1,0:T(8,128)(2,1)} %shard_map.100) | data formatting | bytes 131072

commit v5 on v4

--- a/solution.py
+++ b/solution.py
@@ -45,13 +45,13 @@
         c = self.arrays[kind].at[self.me2(kind), at]
         step = (1 - 2 * way) * (s + 1 if self.direct else 1)
         return pltpu.make_async_remote_copy(
-            src_ref=c, dst_ref=c, send_sem=self.send.at[kind, 0], recv_sem=self.near.at[kind, way, s],
+            src_ref=c, dst_ref=c, send_sem=self.send.at[kind, 0], recv_sem=self.near.at[s],
             device_id=self.device(kind == 0, step), device_id_type=MESH)
 
-    def far_copy(self, kind, way, s, at2, at1):
-        c = self.arrays[kind].at[at2, pl.ds(2 * at1, 2)]
+    def far_copy(self, kind, way, s, j, at2):
+        c = self.arrays[kind].at[at2, pl.ds(2 * self.place(kind, j), 2)]
         return pltpu.make_async_remote_copy(
-            src_ref=c, dst_ref=c, send_sem=self.send.at[kind, 1], recv_sem=self.far.at[kind, way, s, at1],
+            src_ref=c, dst_ref=c, send_sem=self.send.at[kind, 1], recv_sem=self.far.at[s, j],
             device_id=self.device(kind == 1, 1 - 2 * way), device_id_type=MESH)
 
     def place(self, kind, j):
@@ -63,7 +63,7 @@
     def open_chunk(self, j):
         for kind in range(2):
             for way in range(2):
-                self.far_copy(kind, way, 0, self.me2(kind), self.place(kind, j)).start()
+                self.far_copy(kind, way, 0, j, self.me2(kind)).start()
 
     def begin(self):
         for s in range(4 if self.direct else 1):
@@ -71,24 +71,28 @@
                 for way in range(2 if s < 3 else 1):
                     self.near_copy(kind, way, s, self.me1(kind)).start()
 
+    def arrived(self, sem, shards):
+        part = self.arrays[0].at[0, 0:shards]
+        pltpu.make_async_remote_copy(
+            src_ref=part, dst_ref=part, send_sem=self.send.at[0, 0], recv_sem=sem,
+            device_id=self.device(True, 1), device_id_type=MESH).wait_recv()
+
     def near_step(self, u):
-        for way in range(2 if u < 4 else 1):
+        self.arrived(self.near.at[u - 1], 4 if u < 4 else 2)
+        for way in range(2):
             for kind in range(2):
                 at = wrap(self.me1(kind) - u * (1 - 2 * way))
-                self.near_copy(kind, way, u - 1, at).wait_recv()
                 if u < 4 - way and not self.direct:
                     self.near_copy(kind, way, u, at).start()
         self.open_chunk(u - 1)
 
     def far_step(self, s, j):
+        self.arrived(self.far.at[s - 1, j], 8 if s < 4 else 4)
         for way in range(2):
             for kind in range(2):
-                at1 = self.place(kind, j)
                 at2 = wrap(self.me2(kind) - s * (1 - 2 * way))
-                if s < 4 or j % 2 == way:
-                    self.far_copy(kind, way, s - 1, at2, at1).wait_recv()
                 if s < 3 or (s == 3 and j % 2 == way):
-                    self.far_copy(kind, way, s, at2, at1).start()
+                    self.far_copy(kind, way, s, j, at2).start()
 
     def far_steps(self, s):
         for j in range(4):
@@ -99,7 +103,7 @@
             for i, part in enumerate((self.arrays[kind].at[0, 0:7], self.arrays[kind].at[0:7])):
                 pltpu.make_async_remote_copy(
                     src_ref=part, dst_ref=part, send_sem=self.send.at[kind, i],
-                    recv_sem=self.near.at[kind, 0, 0],
+                    recv_sem=self.near.at[0],
                     device_id=self.device(True, 1), device_id_type=MESH).wait_send()
 
 
@@ -109,7 +113,7 @@
     kv_a, kv_b, up_a, up_b, dn_a, dn_b, res_ref, ow_ref, q_all, st_all, ho_all, an_all, sq_all,
     pre_out, pre_in, rs_out, rs_all, keep, o_scr, mix_a, mix_b, got_a, got_b,
     kv_send, kv_near, kv_far, u_send, u_near, u_far, d_send, d_near, d_far,
-    x_send, x_recv, pre_send, pre_recv, in_sem,
+    x_send, x_recv, x_chip, pre_send, pre_recv, in_sem,
 ):
     sp, tp = lax.axis_index("sp"), lax.axis_index("tp")
     z, y = lax.div(sp, RING), lax.rem(sp, RING)
@@ -145,8 +149,6 @@
     ]
     for load in loads:
         load.start()
-    for load in loads:
-        load.wait()
     pl.semaphore_wait(barrier, TP - 1 + 2 * (RING - 1))
 
     def chip(step):
@@ -155,32 +157,33 @@
     def tp_of(step):
         return chip(step) * 2 + c
 
-    def x_copy(k, src, dst, slot, peer):
+    def x_copy(k, src, dst, slot, peer, sem=None):
         return pltpu.make_async_remote_copy(
-            src_ref=src, dst_ref=dst.at[slot], send_sem=x_send.at[k], recv_sem=x_recv.at[k, slot],
-            device_id=(sp, peer), device_id_type=MESH)
-
-    def x_arrived(k, dst, slot):
-        x_copy(k, dst.at[slot], dst, slot, partner).wait_recv()
+            src_ref=src, dst_ref=dst.at[slot], send_sem=x_send.at[k],
+            recv_sem=x_recv.at[k] if sem is None else sem, device_id=(sp, peer), device_id_type=MESH)
+
+    def x_all(k, part):
+        pltpu.make_async_remote_copy(
+            src_ref=part, dst_ref=part, send_sem=x_send.at[k], recv_sem=x_recv.at[k],
+            device_id=(sp, partner), device_id_type=MESH).wait_recv()
 
     def share(k, array):
         for step in (2, 1, 3):
-            x_copy(k, array.at[tp], array, tp, tp_of(step)).start()
+            x_copy(k, array.at[tp], array, tp, tp_of(step), x_chip.at[k % 4, x]).start()
         x_copy(k, array.at[tp], array, tp, partner).start()
 
     def relay(k, array):
         for step in (1, 3, 2):
             slot = tp_of(step)
-            x_arrived(k, array, slot)
+            x_copy(k, array.at[slot], array, slot, partner, x_chip.at[k % 4, chip(step)]).wait_recv()
             x_copy(k, array.at[slot], array, slot, partner).start()
 
     def collect(k, array):
-        for step in (0, 1, 3, 2):
-            x_arrived(k, array, chip(step) * 2 + 1 - c)
+        x_all(k, array.at[0:4])
 
     def x_sent(k, part):
         pltpu.make_async_remote_copy(
-            src_ref=part, dst_ref=part, send_sem=x_send.at[k], recv_sem=x_recv.at[k, 0],
+            src_ref=part, dst_ref=part, send_sem=x_send.at[k], recv_sem=x_recv.at[k],
             device_id=(sp, partner), device_id_type=MESH).wait_send()
 
     events = [(w1, 1, j) for j in range(4)]
@@ -199,18 +202,23 @@
             else:
                 gather.far_step(s, j)
 
+    for load in loads[0:5]:
+        load.wait()
     kv.begin()
     share(0, q_all)
+    for load in loads[5:11]:
+        load.wait()
     w1.begin()
     for u in range(1, 5):
         kv.near_step(u)
-    relay(0, q_all)
     for s in range(1, 4):
         kv.far_steps(s)
+        if s == 1:
+            relay(0, q_all)
         w1.near_step(s)
-    w1.near_step(4)
     w2.begin()
     kv.far_steps(4)
+    w1.near_step(4)
     collect(0, q_all)
 
     lane = lax.broadcasted_iota(jnp.int32, (ROWS, 128), 1)
@@ -241,10 +249,7 @@
             x_copy(1, st_all.at[tp], st_all, tp, chip(step) * 2 + core).start()
     x_copy(1, st_all.at[tp], st_all, tp, partner).start()
     pump(3)
-    x_arrived(1, st_all, partner)
-    for step in (1, 3, 2):
-        for core in range(2):
-            x_arrived(1, st_all, chip(step) * 2 + core)
+    x_all(1, st_all.at[0:7])
 
     every = st_all[...]
     maxima, totals = every[:, 0:16], every[:, 16:32]
@@ -284,10 +289,9 @@
         x_copy(2, rs_out.at[i], rs_all, x, tp_of(step)).start()
     difference = keep[x] + pre_in[x].astype(F32)
     pump(5)
+    x_all(2, rs_all.at[0:3])
     for step in (1, 3, 2):
-        i = chip(step)
-        x_arrived(2, rs_all, i)
-        difference += rs_all[i].astype(F32)
+        difference += rs_all[chip(step)].astype(F32)
 
     square = jnp.mean(difference * difference, axis=-1, keepdims=True)
     ho_all[tp] = (difference * lax.rsqrt(square + EPSILON) * hgain_ref[...]).astype(BF16)
@@ -305,14 +309,14 @@
     squares = jnp.sum(after_mix * after_mix, axis=1, keepdims=True)
     sq_all[tp] = jnp.transpose(jnp.broadcast_to(squares, (ROWS, 128)))[0:8]
     pump(1)
-    share(4, an_all)
-    share(5, sq_all)
+    share(9, an_all)
+    share(10, sq_all)
     pump(4)
-    relay(4, an_all)
-    relay(5, sq_all)
-    pump(1)
-    collect(4, an_all)
-    collect(5, sq_all)
+    relay(9, an_all)
+    relay(10, sq_all)
+    pump(1)
+    collect(9, an_all)
+    collect(10, sq_all)
     squares = jnp.sum(sq_all[...], axis=0)
     squares = jnp.transpose(jnp.broadcast_to(squares[0:1], (128, 128)))[:, 0:1]
     scale = lax.rsqrt(squares / D + EPSILON)
@@ -356,22 +360,13 @@
     def b_copy(k, t, part):
         return pltpu.make_async_remote_copy(
             src_ref=mix_b.at[t, part], dst_ref=got_b.at[tp, part], send_sem=x_send.at[k],
-            recv_sem=x_recv.at[k, tp], device_id=(sp, t), device_id_type=MESH)
+            recv_sem=x_recv.at[k], device_id=(sp, t), device_id_type=MESH)
 
     def give_b(k, part):
         for step in (2, 1, 3):
             for core in range(2):
                 b_copy(k, chip(step) * 2 + core, part).start()
         b_copy(k, partner, part).start()
-
-    def got_part(k, part):
-        @pl.loop(1, TP)
-        def _(p):
-            slot = wrap(tp - p)
-            there = got_b.at[slot, part]
-            pltpu.make_async_remote_copy(
-                src_ref=there, dst_ref=there, send_sem=x_send.at[k], recv_sem=x_recv.at[k, slot],
-                device_id=(sp, partner), device_id_type=MESH).wait_recv()
 
     offsets = (0, 1, -1, 2, -2, 3, -3, 4)
     early, late = pl.ds(0, 7), pl.ds(7, 1)
@@ -395,9 +390,7 @@
     give_b(8, late)
     got_b[tp] = mix_b[tp]
 
-    @pl.loop(1, TP)
-    def _(p):
-        x_arrived(6, got_a, wrap(tp - p))
+    x_all(6, got_a.at[0:7])
 
     source = lax.broadcasted_iota(jnp.int32, (128, 256), 0)
     target = lax.broadcasted_iota(jnp.int32, (128, 256), 1)
@@ -413,8 +406,8 @@
     at = y + lax.div(d + 1, 2) * (2 * lax.rem(d, 2) - 1)
     at = lax.rem(at + RING, RING) * 32 + 16 + lax.rem(source, 16)
     spread = jnp.where(at == target, 1.0, 0.0).astype(BF16)
-    got_part(7, early)
-    got_part(8, late)
+    x_all(7, got_b.at[0:7, 0:7])
+    x_all(8, got_b.at[0, 0:7])
     total = jnp.dot(
         jnp.concatenate([spread] * TP, axis=1), got_b[...].reshape(TP * 128, 128), preferred_element_type=F32)
     out_ref[...] = (keep[0] + jnp.transpose(total)).astype(BF16)
@@ -422,7 +415,7 @@
     kv.finish()
     w1.finish()
     w2.finish()
-    for k, array in ((0, q_all), (1, st_all), (3, ho_all), (4, an_all), (5, sq_all), (6, mix_a)):
+    for k, array in ((0, q_all), (1, st_all), (3, ho_all), (9, an_all), (10, sq_all), (6, mix_a)):
         x_sent(k, array.at[0:7])
     x_sent(2, rs_out.at[0:3])
     x_sent(7, mix_b.at[0:7, 0:7])
@@ -466,10 +459,10 @@
             pltpu.VMEM((TP, 8, 16, 128), BF16),
             pltpu.VMEM(half, BF16),
             pltpu.VMEM((TP, 8, 16, 128), BF16),
-            dma((2, 2)), dma((2, 2, 4)), dma((2, 2, 4, 4)),
-            dma((2, 2)), dma((2, 2, 4)), dma((2, 2, 4, 4)),
-            dma((2, 2)), dma((2, 2, 4)), dma((2, 2, 4, 4)),
-            dma((9,)), dma((9, TP)), dma, dma, dma((11,)),
+            dma((2, 2)), dma((4,)), dma((4, 4)),
+            dma((2, 2)), dma((4,)), dma((4, 4)),
+            dma((2, 2)), dma((4,)), dma((4, 4)),
+            dma((11,)), dma((11,)), dma((4, 4)), dma, dma, dma((11,)),
         ],
         compiler_params=pltpu.CompilerParams(
             collective_id=0, has_side_effects=True, vmem_limit_bytes=67043328),

time: 89.3 us -> 87.4 us (0.979)
  Pallas kernels: 87.6 us -> 85.7 us
    pallas_call x1, Pallas kernels: 87.6 us -> 85.7 us  [on_device(): pl.pallas_call(kernel, out_shape=jax.ShapeDtypeStruct((ROWS, 256), BF16),...]
where the time goes in v5:
time: 87.4 us; the launch traced here: 87.2 us
  Pallas kernels  85.7 us (98%)
  local copies, waits for them, and re-layouts  1.47 us (2%)
    pallas_call x1, Pallas kernels, on_device(): pl.pallas_call(kernel, out_shape=jax.ShapeDtypeStruct((ROWS, 256), BF16),...  85.7 us

profile of v5, /device:TPU:1, one launch (start us, length us, event | category | flops | bytes accessed | tf_op | source)
XLA Modules:
  0.0 87.2 jit_solution(17157324395313708954)
XLA Ops:
  0.0 85.7 %shard_map.100 = bf16[128,256]{1,0:T(8,128)(2,1)} custom-call(f32[8]{0:T(128)} %lam_ref.1, f32[1,256]{1,0:T(1,128)} %bitcast.4, f32[1,256]{1,0:T(1,128)} %bitcast.5, bf16[128,256]{1,0:T(8,128)(2,1)} %res_hbm.1, bf16[128,256]{1,0:T(8,128)(2,1)} %q_hbm.1, bf16[16,512]{1,0:T(8,128)(2,1)} %key_hbm.1, bf16[16,512]{1,0:T(8,128)(2,1)} %val_hbm.1, ...), custom_call_target="tpu_custom_call" | custom-call | tf_op jit(solution)/shard_map/pallas_call | solution.py:433
  85.7 1.5 %copy.12 = bf16[128,256]{1,0:T(8,128)(2,1)} copy(bf16[128,256]{1,0:T(8,128)(2,1)} %shard_map.100) | data formatting | bytes 131072

commit v6 on v5

--- a/solution.py
+++ b/solution.py
@@ -24,11 +24,11 @@
 
 
 class Gather:
-    def __init__(self, first, second, y, z, tp, sems, direct):
+    def __init__(self, first, second, y, z, tp, sems, direct, long=0):
         self.arrays = (first, second)
         self.y, self.z, self.tp = y, z, tp
         self.send, self.near, self.far = sems
-        self.direct = direct
+        self.direct, self.long = direct, long
 
     def me1(self, kind):
         return self.y if kind == 0 else self.z
@@ -68,7 +68,7 @@
     def begin(self):
         for s in range(4 if self.direct else 1):
             for kind in range(2):
-                for way in range(2 if s < 3 else 1):
+                for way in range(2) if s < 3 else (self.long,):
                     self.near_copy(kind, way, s, self.me1(kind)).start()
 
     def arrived(self, sem, shards):
@@ -82,7 +82,7 @@
         for way in range(2):
             for kind in range(2):
                 at = wrap(self.me1(kind) - u * (1 - 2 * way))
-                if u < 4 - way and not self.direct:
+                if u < (4 if way == self.long else 3) and not self.direct:
                     self.near_copy(kind, way, u, at).start()
         self.open_chunk(u - 1)
 
@@ -121,7 +121,7 @@
     partner = x * 2 + 1 - c
     kv = Gather(kv_a, kv_b, y, z, tp, (kv_send, kv_near, kv_far), True)
     w1 = Gather(up_a, up_b, y, z, tp, (u_send, u_near, u_far), False)
-    w2 = Gather(dn_a, dn_b, y, z, tp, (d_send, d_near, d_far), False)
+    w2 = Gather(dn_a, dn_b, y, z, tp, (d_send, d_near, d_far), False, 1)
 
     barrier = pltpu.get_barrier_semaphore()
 

time: 87.4 us -> 86.9 us (level)
  no operation moved by 1% of the time
where the time goes in v6:
time: 86.9 us; the launch traced here: 86.8 us
  Pallas kernels  85.3 us (98%)
  local copies, waits for them, and re-layouts  1.47 us (2%)
    pallas_call x1, Pallas kernels, on_device(): pl.pallas_call(kernel, out_shape=jax.ShapeDtypeStruct((ROWS, 256), BF16),...  85.3 us

profile of v6, /device:TPU:1, one launch (start us, length us, event | category | flops | bytes accessed | tf_op | source)
XLA Modules:
  0.0 86.8 jit_solution(1842357826220991104)
XLA Ops:
  0.0 85.3 %shard_map.100 = bf16[128,256]{1,0:T(8,128)(2,1)} custom-call(f32[8]{0:T(128)} %lam_ref.1, f32[1,256]{1,0:T(1,128)} %bitcast.4, f32[1,256]{1,0:T(1,128)} %bitcast.5, bf16[128,256]{1,0:T(8,128)(2,1)} %res_hbm.1, bf16[128,256]{1,0:T(8,128)(2,1)} %q_hbm.1, bf16[16,512]{1,0:T(8,128)(2,1)} %key_hbm.1, bf16[16,512]{1,0:T(8,128)(2,1)} %val_hbm.1, ...), custom_call_target="tpu_custom_call" | custom-call | tf_op jit(solution)/shard_map/pallas_call | solution.py:433
  85.3 1.5 %copy.12 = bf16[128,256]{1,0:T(8,128)(2,1)} copy(bf16[128,256]{1,0:T(8,128)(2,1)} %shard_map.100) | data formatting | bytes 131072
